TPU v7x, 128 devices: a whole 4x4x4 slice. The times are simulated.
128 devices in a mesh: sp: 16 (over z, y), tp: 8 (over x, core).
Axes of the slice: x: 4, y: 4, z: 4, core: 2. Of those that a mesh axis runs over, the one named last changes fastest.
Arguments:
- resid: bfloat16 [24576, 2048], P(('sp', 'tp')), may hold values from -6 to 6
- cond: bfloat16 [2048], P('sp'), may hold values from -6 to 6
- mod_shift: bfloat16 [2048, 2048], P('sp', 'tp'), may hold values from -0.125 to 0.125
- mod_scale: bfloat16 [2048, 2048], P('sp', 'tp'), may hold values from -0.125 to 0.125
- mod_gate: bfloat16 [2048, 2048], P('sp', 'tp'), may hold values from -0.125 to 0.125
- norm_gain: float32 [2048], replicated, may hold values from 0.1 to 1.9
- context: bfloat16 [1024, 2048], P('sp'), may hold values from -6 to 6
- w_query: bfloat16 [2048, 2048], P(None, 'tp'), may hold values from -0.125 to 0.125
- w_key: bfloat16 [2048, 2048], P(None, 'tp'), may hold values from -0.125 to 0.125
- w_value: bfloat16 [2048, 2048], P(None, 'tp'), may hold values from -0.125 to 0.125
- query_gain: float32 [128], replicated, may hold values from 0.5 to 6, as said below
- key_gain: float32 [128], replicated, may hold values from 0.5 to 6, as said below
- offset_bias: float32 [16, 15, 31], P('tp'), may hold values from -4 to 4
- context_bias: float32 [16], P('tp'), may hold values from -4.5 to 1
- w_out: bfloat16 [2048, 2048], replicated, may hold values from -0.5 to 0.5
Outputs:
- mixed: bfloat16 [24576, 2048], P(('sp', 'tp'))
Inputs may be any that keep to these rules, and one draw needn't show every extreme that they name: `query_gain`: positive gains. `key_gain`: positive gains.
All inputs are finite; a program needn't handle non-finite values.
Results may differ from a plain program's by a relative error of at most 0.0085.
The roundings to bfloat16 on the way count: a program that leaves them out, or rounds other values in their place, can miss the bound.
Values may be sent and summed in bfloat16 or wider, within the bound.
A program may use at most 128 MiB of HBM per device.

v0:
```python
import functools

import jax
import jax.numpy as jnp
from jax import lax
from jax.sharding import Mesh
from jax.sharding import PartitionSpec as P

HEAD_DIM = 128
GRID_W = 64
WIN_ROWS = 8
WIN_COLS = 16
R_DEV = 24
SP = ("sp_0", "sp_1")
SP_TP = ("sp_0", "sp_1", "tp")


EPS = 1e-06


def over_axes(shard, axes):
    return functools.reduce(lax.psum, axes, shard)


def gather_turned(arrays, axis, dims):
    turned = [jnp.moveaxis(a, dim, 0) for a, dim in zip(arrays, dims)]
    widths = [t[0].size for t in turned]
    both = jnp.concatenate([t.reshape(-1, w) for t, w in zip(turned, widths)], axis=1)
    filled = lax.all_gather(both, axis, axis=0, tiled=True)
    blocks = jnp.split(filled, [sum(widths[:k]) for k in range(1, len(widths))], axis=1)
    return tuple(
        (
            jnp.moveaxis(b.reshape(-1, *t.shape[1:]), 0, dim)
            for b, t, dim in zip(blocks, turned, dims)
        )
    )


def side_by_side(arrays, axis, dim, along):
    both = jnp.concatenate(arrays, axis=along)
    filled, at, done = (lax.all_gather(both, axis, axis=dim, tiled=True), 0, [])
    for a in arrays:
        done.append(lax.slice_in_dim(filled, at, at + a.shape[along], axis=along))
        at += a.shape[along]
    return tuple(done)


def padded_2(cells, sides, width):
    for axis, dim in sides:
        count = lax.axis_size(axis)
        ends = count - 1
        head = lax.slice_in_dim(cells, 0, width, axis=dim)
        tail = lax.slice_in_dim(cells, cells.shape[dim] - width, cells.shape[dim], axis=dim)
        cells = jnp.concatenate(
            [
                lax.ppermute(tail, axis, [(i, (i + 1) % count) for i in range(ends)]),
                cells,
                lax.ppermute(head, axis, [((i + 1) % count, i) for i in range(ends)]),
            ],
            axis=dim,
        )
    return cells


def head_norm(values, gain, heads_local):
    count = values.shape[0]
    split = values.reshape(count, heads_local, -1)
    scaled = split * lax.rsqrt(jnp.mean(split * split, axis=-1, keepdims=True) + EPS) * gain
    return scaled.reshape(count, -1).astype(jnp.bfloat16)


def project_context(rows_in, norm_gain, w_key, w_value, key_gain, heads_local):
    floats = rows_in.astype(jnp.float32)
    inverse = lax.rsqrt(jnp.mean(floats * floats, axis=-1, keepdims=True) + EPS)
    normed = (floats * inverse * norm_gain).astype(jnp.bfloat16)
    keys = head_norm(
        jnp.dot(normed, w_key, preferred_element_type=jnp.float32), key_gain, heads_local
    )
    values = jnp.dot(normed, w_value, preferred_element_type=jnp.float32).astype(jnp.bfloat16)
    return (keys, values)


def attend_rows(
    queries, key_at, value_at, row_offset, offset_bias, ctx_key, ctx_value, context_bias
):
    grid_w = queries.shape[1]
    columns = jnp.arange(grid_w, dtype=jnp.int32)
    col_begin = jnp.clip(columns - WIN_COLS // 2, 0, grid_w - WIN_COLS)
    valid = (columns[None, :] >= col_begin[:, None]) & (
        columns[None, :] < col_begin[:, None] + WIN_COLS
    )
    col_offset = jnp.clip(columns[None, :] - columns[:, None] + WIN_COLS - 1, 0, 2 * WIN_COLS - 2)
    col_onehot = (col_offset[..., None] == jnp.arange(2 * WIN_COLS - 1, dtype=jnp.int32)).astype(
        jnp.float32
    )
    row_onehot = (
        row_offset[:, :, None] == jnp.arange(2 * WIN_ROWS - 1, dtype=jnp.int32)[None, None, :]
    ).astype(jnp.float32)
    bias = jnp.einsum(
        "nir,hrj,ckj->nhcik", row_onehot, offset_bias, col_onehot, precision=lax.Precision.HIGHEST
    )
    factor = HEAD_DIM ** (-0.5)
    s_win = (
        jnp.stack(
            [
                jnp.einsum(
                    "nchd,nkhd->nhck", queries, key_at(i), preferred_element_type=jnp.float32
                )
                for i in range(WIN_ROWS)
            ],
            axis=3,
        )
        * factor
        + bias
    )
    s_win = jnp.where(valid[None, None, :, None, :], s_win, -1e30)
    s_ctx = (
        jnp.einsum("nchd,jhd->nhcj", queries, ctx_key, preferred_element_type=jnp.float32) * factor
    )
    s_ctx = s_ctx + context_bias[None, :, None, None]
    top = jnp.maximum(jnp.max(s_win, axis=(3, 4)), jnp.max(s_ctx, axis=3))
    e_win = jnp.exp(s_win - top[..., None, None])
    e_ctx = jnp.exp(s_ctx - top[..., None])
    total = jnp.sum(e_win, axis=(3, 4)) + jnp.sum(e_ctx, axis=3)
    p_win = (e_win / total[..., None, None]).astype(jnp.bfloat16)
    p_ctx = (e_ctx / total[..., None]).astype(jnp.bfloat16)
    out = jnp.einsum("nhcj,jhd->nchd", p_ctx, ctx_value, preferred_element_type=jnp.float32)
    for i in range(WIN_ROWS):
        out = out + jnp.einsum(
            "nhck,nkhd->nchd", p_win[:, :, :, i], value_at(i), preferred_element_type=jnp.float32
        )
    count = queries.shape[0]
    return out.astype(jnp.bfloat16).reshape(count * grid_w, -1)


def shards(
    resid,
    cond,
    mod_shift,
    mod_scale,
    mod_gate,
    norm_gain,
    context,
    w_query,
    w_key,
    w_value,
    query_gain,
    key_gain,
    offset_bias,
    context_bias,
    w_out,
):
    heads_local = offset_bias.shape[0]
    width = w_query.shape[1]
    lifted = jax.nn.silu(cond.astype(jnp.float32)).astype(jnp.bfloat16)
    shift_part = jnp.dot(lifted, mod_shift, preferred_element_type=jnp.float32)
    scale_part = jnp.dot(lifted, mod_scale, preferred_element_type=jnp.float32)
    gate_part = jnp.dot(lifted, mod_gate, preferred_element_type=jnp.float32)
    summed = (over_axes(shift_part, SP), over_axes(scale_part, SP), over_axes(gate_part, SP))
    shift, scale, gate = gather_turned((summed[0], summed[1], summed[2]), "tp", (0, 0, 0))
    floats = resid.astype(jnp.float32)
    inverse = lax.rsqrt(jnp.mean(floats * floats, axis=-1, keepdims=True) + EPS)
    normed = (floats * inverse * norm_gain * (1.0 + scale) + shift).astype(jnp.bfloat16)
    piece = lax.all_gather(normed, "tp", axis=0, tiled=True)
    queries = head_norm(
        jnp.dot(piece, w_query, preferred_element_type=jnp.float32), query_gain, heads_local
    )
    keys = head_norm(
        jnp.dot(piece, w_key, preferred_element_type=jnp.float32), key_gain, heads_local
    )
    values = jnp.dot(piece, w_value, preferred_element_type=jnp.float32).astype(jnp.bfloat16)
    projected = jnp.concatenate([queries, keys, values], axis=1)
    query = projected[:, :width]
    key_value = projected[:, width:]
    own_key, own_value = project_context(context, norm_gain, w_key, w_value, key_gain, heads_local)
    ctx_key, ctx_value = side_by_side((own_key, own_value), SP, 0, 1)
    ctx_count = ctx_key.shape[0]
    ctx_key = ctx_key.reshape(ctx_count, heads_local, HEAD_DIM)
    ctx_value = ctx_value.reshape(ctx_count, heads_local, HEAD_DIM)
    reach = WIN_ROWS // 2
    grid = key_value.reshape(R_DEV, GRID_W, 2 * width)
    padded = padded_2(grid, ((SP, 0),), reach)
    padded = padded.reshape(R_DEV + 2 * reach, GRID_W, 2, heads_local, HEAD_DIM)
    total_rows = R_DEV * lax.axis_size(SP)
    first = lax.axis_index(SP) * R_DEV
    global_rows = first + jnp.arange(R_DEV, dtype=jnp.int32)
    row_start = jnp.clip(global_rows - reach, 0, total_rows - WIN_ROWS)
    window_rows = jnp.arange(WIN_ROWS, dtype=jnp.int32)[None, :]
    row_offset = row_start[:, None] + window_rows - global_rows[:, None] + WIN_ROWS - 1
    queries = query.reshape(R_DEV, GRID_W, heads_local, HEAD_DIM)
    upper = min(reach, R_DEV)
    lower = max(upper, R_DEV - reach)
    edge_rows = list(range(upper)) + list(range(lower, R_DEV))
    edge_index = jnp.array(edge_rows, dtype=jnp.int32)
    edge_window = (jnp.take(row_start, edge_index) - first + reach)[:, None] + window_rows
    edge_kv = jnp.take(padded, edge_window, axis=0)
    edge_out = attend_rows(
        jnp.take(queries, edge_index, axis=0),
        lambda i: edge_kv[:, i, :, 0],
        lambda i: edge_kv[:, i, :, 1],
        jnp.take(row_offset, edge_index, axis=0),
        offset_bias,
        ctx_key,
        ctx_value,
        context_bias,
    )
    pieces = [edge_out[: upper * GRID_W]]
    middle = lower - upper
    inner_out = attend_rows(
        queries[upper:lower],
        lambda i: padded[upper + i : upper + i + middle, :, 0],
        lambda i: padded[upper + i : upper + i + middle, :, 1],
        row_offset[upper:lower],
        offset_bias,
        ctx_key,
        ctx_value,
        context_bias,
    )
    pieces.append(inner_out)
    pieces.append(edge_out[upper * GRID_W :])
    attended = jnp.concatenate(pieces, axis=0)
    full_rows = lax.all_to_all(attended, "tp", split_axis=0, concat_axis=1, tiled=True)
    result = jnp.dot(full_rows, w_out, preferred_element_type=jnp.float32)
    return (floats + gate * result).astype(jnp.bfloat16)


def solution(mesh):
    split = Mesh(mesh.devices.reshape(4, 4, mesh.shape["tp"]), ("sp_0", "sp_1", "tp"))
    placed = (
        P(SP_TP, None),
        P(SP),
        P(SP, "tp"),
        P(SP, "tp"),
        P(SP, "tp"),
        P(),
        P(SP, None),
        P(None, "tp"),
        P(None, "tp"),
        P(None, "tp"),
        P(),
        P(),
        P("tp", None, None),
        P("tp"),
        P(),
    )
    return jax.shard_map(
        shards, mesh=split, in_specs=placed, out_specs=P(SP_TP, None), check_vma=False
    )
```

profile of v0, /device:TPU:1, one launch (start us, length us, event | category | flops | bytes accessed | tf_op | source)
XLA Modules:
  0.0 245.1 jit_solution(12134459745243298402)
XLA Ops:
  10.0 1.7 convolution_convert_fusion.1
  15.5 10.5 %all-reduce.1 = (f32[256]{0:T(256)S(1)}, f32[256]{0:T(256)S(1)}, f32[256]{0:T(256)S(1)}) all-reduce(f32[256]{0:T(256)S(1)} %bitcast.451, f32[256]{0:T(256)S(1)} %bitcast.450, f32[256]{0:T(256)S(1)} %bitcast.449), channel_id=1, replica_groups=mesh['sp_0'=4,'sp_1'=4,'tp'=8] {'sp_0'}, use_global_device_ids=true, to_apply=%region_4.5 | all-reduce | flops 768 | bytes 6144 | tf_op jit(solution)/shard_map/psum | solution.py:22
  26.1 9.0 %all-reduce = (f32[256,1]{0,1:T(1,128)S(1)}, f32[256,1]{0,1:T(1,128)S(1)}, f32[256,1]{0,1:T(1,128)S(1)}) all-reduce(f32[256,1]{0,1:T(1,128)S(1)} %bitcast.452, f32[256,1]{0,1:T(1,128)S(1)} %bitcast.453, f32[256,1]{0,1:T(1,128)S(1)} %bitcast.454), channel_id=1, replica_groups=mesh['sp_0'=4,'sp_1'=4,'tp'=8] {'sp_1'}, use_global_device_ids=true, to_apply=%region_5.6 | all-reduce | flops 768 | bytes 6144 | tf_op jit(solution)/shard_map/psum | solution.py:22
  35.0 17.6 %all_gather.9 = f32[2048,3]{0,1:T(4,128)S(1)} all-gather(f32[256,3]{0,1:T(4,128)S(1)} %pad_maximum_fusion.4), channel_id=1, replica_groups=mesh['sp_0'=4,'sp_1'=4,'tp'=8] {'tp'}, dimensions={0}, use_global_device_ids=true | all-gather | bytes 27648 | tf_op jit(solution)/shard_map/all_gather | solution.py:29
  56.2 5.8 %fusion.111 = f32[64,64,2,16,8]{1,3,4,2,0:T(8,128)} fusion(f32[64,64,2,15,1]{1,3,4,2,0:T(8,128)S(1)} %convolution_bitcast_fusion.16, s32[16,8]{0,1:T(8,128)S(1)} %copy.538), kind=kOutput, calls=%fused_computation.234 | convolution fusion | flops 188745600 | bytes 4686336 | tf_op jit(solution)/shard_map/nir,hrj,ckj->nhcik/dot_general | solution.py:99
  62.0 9.7 %copy.539 = f32[64,64,2,16,8]{0,1,2,3,4:T(8,128)} copy(f32[64,64,2,16,8]{1,3,4,2,0:T(8,128)} %fusion.111) | data formatting | bytes 8388608 | tf_op jit(solution)/shard_map/nir,hrj,ckj->nhcik/dot_general | solution.py:99
  71.9 3.8 %fusion.116 = f32[64,64,2,8,8]{1,4,3,2,0:T(8,128)} fusion(f32[64,64,2,15,1]{1,3,4,2,0:T(8,128)S(1)} %convolution_bitcast_fusion.16, s32[8,8]{1,0:T(8,128)S(1)} %gather_fusion.3), kind=kOutput, calls=%fused_computation.243 | convolution fusion | flops 94372800 | bytes 2588928 | tf_op jit(solution)/shard_map/nir,hrj,ckj->nhcik/dot_general | solution.py:99
  75.7 5.7 %copy.496 = f32[64,64,2,8,8]{0,1,2,3,4:T(8,128)} copy(f32[64,64,2,8,8]{1,4,3,2,0:T(8,128)} %fusion.116) | data formatting | bytes 4194304 | tf_op jit(solution)/shard_map/nir,hrj,ckj->nhcik/dot_general | solution.py:99
  81.5 2.1 fusion.140
  84.6 16.2 %all-gather.5.cloned.1.call-done = bf16[1536,2048]{1,0:T(8,128)(2,1)} async-done(((bf16[192,2048]{1,0:T(8,128)(2,1)}), bf16[1536,2048]{1,0:T(8,128)(2,1)}) %all-gather.5.cloned.1.call-update) | async-done | bytes 6291472 | tf_op jit(solution)/shard_map/all_gather | solution.py:164
  100.7 4.8 %bitcast_reduce_fusion.2 = (f32[1536,2]{0,1:T(2,128)S(1)}, f32[1536,256]{0,1:T(8,128)S(1)}) fusion(bf16[1536,2048]{1,0:T(8,128)(2,1)} %all-gather.5.cloned.1.call-done, bf16[2048,256]{1,0:T(8,128)(2,1)S(1)} %copy-done), kind=kOutput, calls=%fused_computation.49 | convolution fusion | flops 1611396096 | bytes 8925184 | tf_op jit(solution)/shard_map/dot_general | solution.py:169
  105.8 1.9 convolution_convert_fusion
  109.4 2.4 concatenate.26
  111.8 8.0 %fusion.139 = (bf16[16,64,1,2,128]{4,3,2,1,0:T(2,128)(2,1)}, bf16[16,64,1,2,128]{4,3,2,1,0:T(2,128)(2,1)}, bf16[16,64,1,2,128]{4,3,2,1,0:T(2,128)(2,1)}, bf16[16...) fusion(bf16[24,64,2,2,128]{4,3,2,1,0:T(2,128)(2,1)S(1)} %concat, ...), kind=kLoop, calls=%fused_computation.286 | loop fusion | bytes 16777216 | tf_op jit(solution)/shard_map/slice | solution.py:212
  119.8 4.7 %bitcast_reduce_fusion.3 = (f32[1536,2]{0,1:T(2,128)S(1)}, f32[1536,256]{0,1:T(8,128)S(1)}) fusion(bf16[1536,2048]{1,0:T(8,128)(2,1)} %all-gather.5.cloned.1.call-done, bf16[2048,256]{1,0:T(8,128)(2,1)S(1)} %copy-done.41), kind=kOutput, calls=%fused_computation.53 | convolution fusion | flops 1611396096 | bytes 8925184 | tf_op jit(solution)/shard_map/dot_general | solution.py:166
  125.8 2.0 copy.519
  134.7 3.3 %copy-done.7 = f32[16,2,64,8,64]{2,4,1,0,3:T(8,128)} copy-done((f32[16,2,64,8,64]{2,4,1,0,3:T(8,128)}, f32[16,2,64,8,64]{2,4,1,0,3:T(8,128)S(1)}, u32[]{:S(2)}) %copy-start.7) | copy-done | bytes 4194328
  139.2 3.2 %copy-done.2 = f32[2,1024,1024]{1,2,0} copy-done((f32[2,1024,1024]{1,2,0}, f32[2,1024,1024]{1,2,0:S(1)}, u32[]{:S(2)}) %copy-start.2) | copy-done | bytes 8388632
  143.4 12.2 %fusion.135 = (f32[16,2,64]{2,1,0:T(2,128)S(1)}, f32[16,2,64,8,64]{2,4,1,0,3:T(8,128)}) fusion(f32[64,64,2,16,8]{0,1,2,3,4:T(8,128)} %copy.539, f32[16,2,64,8,64]{2,4,1,0,3:T(8,128)} %copy-done.7, pred[64,64]{0,1:T(8,128)(4,1)S(1)} %fusion.114), kind=kLoop, calls=%fused_computation.284 | loop fusion | flops 4192256 | bytes 12595200 | tf_op jit(solution)/shard_map/reduce_max | solution.py:121
  155.6 4.5 %fusion.3 = f32[16,2,64]{2,0,1:T(8,128)S(1)} fusion(f32[2,1024,16,64]{1,3,2,0:T(8,128)} %bitcast.426, f32[16,2,64]{2,0,1:T(8,128)S(1)} %copy_maximum_fusion, f32[2]{0:T(128)S(1)} %copy-done.38), kind=kLoop, calls=%fused_computation.14 | loop fusion | flops 8386560 | bytes 8405000 | tf_op jit(solution)/shard_map/reduce_sum | solution.py:124
  164.0 4.8 %fusion.2 = f32[16,2,64]{2,1,0:T(2,128)S(1)} fusion(f32[16,2,64,8,64]{2,4,1,0,3:T(8,128)} %get-tuple-element.12, f32[16,2,64]{2,1,0:T(2,128)S(1)} %copy.541), kind=kLoop, calls=%fused_computation.13 | loop fusion | flops 2095104 | bytes 4210688 | tf_op jit(solution)/shard_map/reduce_sum | solution.py:124
  168.8 4.3 %divide_convert_fusion = bf16[16,2,64,8,64]{2,4,1,0,3:T(8,128)(2,1)S(1)} fusion(f32[16,2,64,8,64]{2,4,1,0,3:T(8,128)} %get-tuple-element.12, f32[16,2,64]{2,1,0:T(2,128)S(1)} %copy.545, f32[16,2,64]{2,1,0:T(2,128)S(1)} %copy.541), kind=kLoop, calls=%fused_computation.9 | loop fusion | flops 3145728 | bytes 6307840 | tf_op jit(solution)/shard_map/convert_element_type | solution.py:125
  173.1 1.8 slice_bitcast_fusion
  176.5 2.2 fusion.21
  184.2 3.8 %collective-permute-start = (bf16[4,64,512]{2,1,0:T(8,128)(2,1)}, bf16[4,64,512]{2,1,0:T(8,128)(2,1)}, u32[]{:S(2)}, u32[]{:S(2)}) collective-permute-start(bf16[4,64,512]{2,1,0:T(8,128)(2,1)} %bitcast.23), channel_id=1, source_target_pairs={{0,8},{8,16},{16,24},{24,32},{32,40},{40,48},{48,56},{56,64},{64,7... | collective-permute-start | bytes 786440 | tf_op jit(solution)/shard_map/ppermute | solution.py:56
  192.7 1.9 copy-done.4
  196.3 2.1 collective-permute-done.1
  199.5 1.7 pad_maximum_fusion
  201.2 3.1 %gather_fusion.2 = bf16[64,64,2,2,128]{4,1,3,2,0:T(8,128)(2,1)} fusion(bf16[32,64,2,2,128]{4,1,3,2,0:T(8,128)(2,1)S(1)} %pad_maximum_fusion, s32[1024]{0:T(1024)S(1)} %pad_clamp_fusion), kind=kCustom, calls=%fused_computation.2 | custom fusion | bytes 8388864 | tf_op jit(solution)/shard_map/jit(_take)/gather | solution.py:196
  204.3 2.6 %copy_select_fusion = bf16[8,8,64,2,2,128]{5,2,4,0,3,1:T(8,128)(2,1)S(1)} fusion(bf16[8,8,64,2,2,128]{5,2,4,3,1,0:T(8,128)(2,1)} %bitcast.431, pred[8,8]{0,1:T(8,128)(4,1)S(1)} %fusion.123), kind=kLoop, calls=%fused_computation.20 | loop fusion | flops 2097152 | bytes 8388672 | tf_op jit(solution)/shard_map/jit(_take)/select_n | solution.py:196
  218.6 16.5 %all_to_all.19 = bf16[8,192,256]{2,1,0:T(8,128)(2,1)S(1)} all-to-all(bf16[8,192,256]{2,1,0:T(8,128)(2,1)S(1)} %bitcast.432), channel_id=1, replica_groups=mesh['sp_0'=4,'sp_1'=4,'tp'=8] {'tp'}, dimensions={0} | all-to-all | bytes 1572864 | tf_op jit(solution)/shard_map/all_to_all | solution.py:222
  235.3 2.7 %fusion.10 = bf16[192,2048]{1,0:T(8,128)(2,1)} fusion(bf16[192,2048]{1,0:T(8,128)(2,1)S(1)} %bitcast.438, bf16[2048,2048]{1,0:T(8,128)(2,1)S(1)} %bitcast.456, bf16[192,2048]{1,0:T(8,128)(2,1)S(1)} %copy-done.13, f32[2048]{0:T(1024)S(1)} %bitcast.448), kind=kOutput, calls=%fused_computation.31 | convolution fusion | flops 1612185600 | bytes 10756096 | tf_op jit(solution)/shard_map/dot_general | solution.py:223
  (212 shorter events, 53.7 us)
Async XLA Ops:
  6.5 47.7 %copy-start.39 = (s32[8]{0:T(128)S(1)}, s32[8]{0:T(128)}, u32[]{:S(2)}) copy-start(s32[8]{0:T(128)} %constant.138) | copy-start | bytes 100
  6.5 46.3 %copy-start.36 = (f32[2048]{0:T(1024)S(1)}, f32[2048]{0:T(1024)}, u32[]{:S(2)}) copy-start(f32[2048]{0:T(1024)} %param.21) | copy-start | bytes 24580
  6.5 46.1 %copy-start.12 = (bf16[192,2048]{1,0:T(8,128)(2,1)S(1)}, bf16[192,2048]{1,0:T(8,128)(2,1)}, u32[]{:S(2)}) copy-start(bf16[192,2048]{1,0:T(8,128)(2,1)} %param.16) | copy-start | bytes 2359300
  6.5 49.0 %copy-start.37 = (f32[2,15,31]{2,0,1:T(2,128)S(1)}, f32[2,15,31]{2,0,1:T(2,128)}, u32[]{:S(2)}) copy-start(f32[2,15,31]{2,0,1:T(2,128)} %param.28) | copy-start | bytes 11164
  6.5 75.0 %all-gather.3.cloned.1.call-start = ((), (), s32[]{:S(2)}) async-start(), calls=%async_computation.1 | async-start | bytes 1114112 | tf_op jit(solution)/shard_map/all_gather | solution.py:41
  12.5 88.2 %all-gather.5.cloned.1.call-start = ((), (), s32[]{:S(2)}) async-start(), calls=%async_computation.2 | async-start | bytes 7077888 | tf_op jit(solution)/shard_map/all_gather | solution.py:164
  75.7 5.7 %copy-start.42 = (f32[128]{0:T(128)S(1)}, f32[128]{0:T(128)}, u32[]{:S(2)}) copy-start(f32[128]{0:T(128)} %param.26) | copy-start | bytes 1540
  84.6 21.2 %copy-start.31 = (bf16[2048,256]{1,0:T(8,128)(2,1)S(1)}, bf16[2048,256]{1,0:T(8,128)(2,1)}, u32[]{:S(2)}) copy-start(bf16[2048,256]{1,0:T(8,128)(2,1)} %param.25) | copy-start | bytes 3145732
  100.7 5.0 %copy-start.40 = (bf16[1536,2048]{1,0:T(8,128)(2,1)S(1)}, bf16[1536,2048]{1,0:T(8,128)(2,1)}, u32[]{:S(2)}) copy-start(bf16[1536,2048]{1,0:T(8,128)(2,1)} %all-gather.5.cloned.1.call-done) | copy-start | bytes 18874372
  107.7 4.1 %copy-start.14 = (bf16[1536,256]{0,1:T(8,128)(2,1)}, bf16[1536,256]{0,1:T(8,128)(2,1)S(1)}, u32[]{:S(2)}) copy-start(bf16[1536,256]{0,1:T(8,128)(2,1)S(1)} %convolution_convert_fusion) | copy-start | bytes 2359300
  111.8 8.0 %copy-start.41 = (bf16[2048,256]{1,0:T(8,128)(2,1)S(1)}, bf16[2048,256]{1,0:T(8,128)(2,1)}, u32[]{:S(2)}) copy-start(bf16[2048,256]{1,0:T(8,128)(2,1)} %param.23) | copy-start | bytes 3145732
  127.8 4.8 %copy-start.29 = (bf16[16,64,1,2,128]{4,3,2,1,0:T(2,128)(2,1)S(1)}, bf16[16,64,1,2,128]{4,3,2,1,0:T(2,128)(2,1)}, u32[]{:S(2)}) copy-start(bf16[16,64,1,2,128]{4,3,2,1,0:T(2,128)(2,1)} %get-tuple-element.50) | copy-start | bytes 1572868
  129.0 3.1 %copy-start.30 = (bf16[16,64,1,2,128]{4,3,2,1,0:T(2,128)(2,1)S(1)}, bf16[16,64,1,2,128]{4,3,2,1,0:T(2,128)(2,1)}, u32[]{:S(2)}) copy-start(bf16[16,64,1,2,128]{4,3,2,1,0:T(2,128)(2,1)} %get-tuple-element.51) | copy-start | bytes 1572868
  129.2 3.8 %copy-start.28 = (bf16[16,64,1,2,128]{4,3,2,1,0:T(2,128)(2,1)S(1)}, bf16[16,64,1,2,128]{4,3,2,1,0:T(2,128)(2,1)}, u32[]{:S(2)}) copy-start(bf16[16,64,1,2,128]{4,3,2,1,0:T(2,128)(2,1)} %get-tuple-element.49) | copy-start | bytes 1572868
  130.7 2.8 %copy-start.27 = (bf16[16,64,1,2,128]{4,3,2,1,0:T(2,128)(2,1)S(1)}, bf16[16,64,1,2,128]{4,3,2,1,0:T(2,128)(2,1)}, u32[]{:S(2)}) copy-start(bf16[16,64,1,2,128]{4,3,2,1,0:T(2,128)(2,1)} %get-tuple-element.48) | copy-start | bytes 1572868
  133.0 4.9 %copy-start.10 = (bf16[128,2,8,128]{3,2,1,0:T(8,128)(2,1)S(1)}, bf16[128,2,8,128]{3,2,1,0:T(8,128)(2,1)}, u32[]{:S(2)}) copy-start(bf16[128,2,8,128]{3,2,1,0:T(8,128)(2,1)} %get-tuple-element.58) | copy-start | bytes 1572868
  134.7 3.3 %copy-start.7 = (f32[16,2,64,8,64]{2,4,1,0,3:T(8,128)}, f32[16,2,64,8,64]{2,4,1,0,3:T(8,128)S(1)}, u32[]{:S(2)}) copy-start(f32[16,2,64,8,64]{2,4,1,0,3:T(8,128)S(1)} %fusion.30) | copy-start | bytes 12582916
  137.9 4.5 %copy-start.38 = (f32[2]{0:T(128)S(1)}, f32[2]{0:T(128)}, u32[]{:S(2)}) copy-start(f32[2]{0:T(128)} %param.29) | copy-start | bytes 28
  139.2 3.2 %copy-start.2 = (f32[2,1024,1024]{1,2,0}, f32[2,1024,1024]{1,2,0:S(1)}, u32[]{:S(2)}) copy-start(f32[2,1024,1024]{1,2,0:S(1)} %fusion.62) | copy-start | bytes 25165828
  155.6 6.2 %copy-start.15 = (bf16[1536,256]{0,1:T(8,128)(2,1)S(1)}, bf16[1536,256]{0,1:T(8,128)(2,1)}, u32[]{:S(2)}) copy-start(bf16[1536,256]{0,1:T(8,128)(2,1)} %copy-done.14) | copy-start | bytes 2359300
  160.2 2.5 %copy-start.9 = (bf16[1536,256]{0,1:T(8,128)(2,1)S(1)}, bf16[1536,256]{0,1:T(8,128)(2,1)}, u32[]{:S(2)}) copy-start(bf16[1536,256]{0,1:T(8,128)(2,1)} %copy-done.8) | copy-start | bytes 2359300
  168.8 6.2 %copy-start.34 = (bf16[1024,2,128]{2,1,0:T(2,128)(2,1)S(1)}, bf16[1024,2,128]{2,1,0:T(2,128)(2,1)}, u32[]{:S(2)}) copy-start(bf16[1024,2,128]{2,1,0:T(2,128)(2,1)} %reshape.300) | copy-start | bytes 1572868
  173.1 3.4 %copy-start.3 = (f32[2,1024,1024]{1,2,0:S(1)}, f32[2,1024,1024]{1,2,0}, u32[]{:S(2)}) copy-start(f32[2,1024,1024]{1,2,0} %copy-done.2) | copy-start | bytes 25165828
  176.5 2.6 %copy-start.23 = (bf16[16,64,1,2,128]{4,3,2,1,0:T(2,128)(2,1)S(1)}, bf16[16,64,1,2,128]{4,3,2,1,0:T(2,128)(2,1)}, u32[]{:S(2)}) copy-start(bf16[16,64,1,2,128]{4,3,2,1,0:T(2,128)(2,1)} %get-tuple-element.44) | copy-start | bytes 1572868
  181.2 6.8 %copy-start.32 = (bf16[256,512]{0,1:T(8,128)(2,1)S(1)}, bf16[256,512]{0,1:T(8,128)(2,1)}, u32[]{:S(2)}) copy-start(bf16[256,512]{0,1:T(8,128)(2,1)} %get-tuple-element.56) | copy-start | bytes 786436
  181.6 10.4 %copy-start.11 = (bf16[128,2,8,128]{3,2,1,0:T(8,128)(2,1)S(1)}, bf16[128,2,8,128]{3,2,1,0:T(8,128)(2,1)}, u32[]{:S(2)}) copy-start(bf16[128,2,8,128]{3,2,1,0:T(8,128)(2,1)} %get-tuple-element.58) | copy-start | bytes 1572868
  184.2 11.0 %collective-permute-start = (bf16[4,64,512]{2,1,0:T(8,128)(2,1)}, bf16[4,64,512]{2,1,0:T(8,128)(2,1)}, u32[]{:S(2)}, u32[]{:S(2)}) collective-permute-start(bf16[4,64,512]{2,1,0:T(8,128)(2,1)} %bitcast.23), channel_id=1, source_target_pairs={{0,8},{8,16},{16,24},{24,32},{32,40},{40,48},{48,56},{56,64},{64,7... | collective-permute-start | bytes 786440 | tf_op jit(solution)/shard_map/ppermute | solution.py:56
  188.9 9.5 %collective-permute-start.1 = (bf16[4,64,512]{2,1,0:T(8,128)(2,1)}, bf16[4,64,512]{2,1,0:T(8,128)(2,1)}, u32[]{:S(2)}, u32[]{:S(2)}) collective-permute-start(bf16[4,64,512]{2,1,0:T(8,128)(2,1)} %bitcast.24), channel_id=1, source_target_pairs={{8,0},{16,8},{24,16},{32,24},{40,32},{48,40},{56,48},{64,56},{72,6... | collective-permute-start | bytes 786440 | tf_op jit(solution)/shard_map/ppermute | solution.py:58
  215.5 19.8 %slice-start = ((s8[8388608]{0:T(1024)(128)(4,1)}), s8[4194304]{0:T(1024)(128)(4,1)S(1)}, s32[]{:S(2)}) async-start(s8[8388608]{0:T(1024)(128)(4,1)} %bitcast.455), calls=%async_computation.3 | async-start | bytes 8388608
  217.4 17.8 %slice-start.1 = ((s8[8388608]{0:T(1024)(128)(4,1)}), s8[4194304]{0:T(1024)(128)(4,1)S(1)}, s32[]{:S(2)}) async-start(s8[8388608]{0:T(1024)(128)(4,1)} %bitcast.455), calls=%async_computation.4 | async-start | bytes 8388608
  218.2 17.1 %copy-start.13 = (bf16[192,2048]{1,0:T(8,128)(2,1)S(1)}, bf16[192,2048]{1,0:T(8,128)(2,1)}, u32[]{:S(2)}) copy-start(bf16[192,2048]{1,0:T(8,128)(2,1)} %param.16) | copy-start | bytes 2359300
  235.3 2.7 %copy-start.1 = (bf16[2048,256]{1,0:T(8,128)(2,1)S(1)}, bf16[2048,256]{1,0:T(8,128)(2,1)}, u32[]{:S(2)}) copy-start(bf16[2048,256]{1,0:T(8,128)(2,1)} %param.24) | copy-start | bytes 3145732
  (17 other events, 27.4 us)
Sparse Core Ops, SparseCore 0:
  12.6 44.1 all-gather.2
  58.5 42.1 all-gather.4
where the time goes:
time: 250 us; the launch traced here: 245 us
  local copies, waits for them, and re-layouts  64 us (26%)
  blocking collectives  53.6 us (21%)
  matrix products  48.4 us (19%)
  other arithmetic  40.8 us (16%)
  waiting for transfers between devices  18.4 us (7%)
  between operations  14.7 us (6%)
  starting transfers between devices  5.16 us (2%)
    psum x2, blocking collectives, over_axes(): return functools.reduce(lax.psum, axes, shard)  19.5 us
    all_gather x1, blocking collectives, gather_turned(): filled = lax.all_gather(both, axis, axis=0, tiled=True)  17.6 us
    all_to_all x1, blocking collectives, shards(): lax.all_to_all(attended, 'tp', split_axis=0, concat_axis=1, tiled=True)  16.5 us
    all_gather x1, waiting for transfers between devices, shards(): piece = lax.all_gather(normed, 'tp', axis=0, tiled=True)  16.2 us
    dot_general x2, local copies, waits for them, and re-layouts, attend_rows(): jnp.einsum('nir,hrj,ckj->nhcik', row_onehot, offset_bias, col_onehot, pre...  15.4 us
    reduce_max x4, other arithmetic, attend_rows(): top = jnp.maximum(jnp.max(s_win, axis=(3, 4)), jnp.max(s_ctx, axis=3))  15.3 us
    unnamed x93, local copies, waits for them, and re-layouts  12 us
    reduce_sum x4, other arithmetic, attend_rows(): total = jnp.sum(e_win, axis=(3, 4)) + jnp.sum(e_ctx, axis=3)  11.1 us
  transfers between devices with their start and end apart: 4, of which 2 were waited for; matrix products, arithmetic and copies ran while one was open for 16% of the time, Pallas kernels for 0%

commit v1 on v0

v1 whole, which is shorter than its diff:
```python
import functools

import jax
import jax.numpy as jnp
from jax import lax
from jax.experimental import pallas as pl
from jax.experimental.pallas import tpu as pltpu
from jax.sharding import Mesh
from jax.sharding import PartitionSpec as P

MESH = pl.DeviceIdType.MESH
BF16, F32 = jnp.bfloat16, jnp.float32
EPS = 1e-06
LOG2E = 1.4426950408889634
HEAD = 128
GRID_W = 64
D = 2048
CTX = 1024
ROWS_DEV = 24
TOK = 1536
SHARD = 192
HALF = 96
WIDE = 256
NEG = -1e30
NT = (((1,), (1,)), ((), ()))


def dot_nt(a, b):
    return lax.dot_general(a, b, NT, preferred_element_type=F32)


def dot(a, b):
    return jnp.dot(a, b, preferred_element_type=F32)


def inv_rms(v):
    return lax.rsqrt(jnp.mean(v * v, axis=-1, keepdims=True) + EPS)


def kernel(
    resid, cond, mod_shift, mod_scale, mod_gate, norm_gain, context, w_query, w_key, w_value,
    query_gain, key_gain, offset_bias, context_bias, w_out, out,
    G, WQ, WK, WV, WO, CX, NRM, R, Q, KV, CKV, MP, MS, MSUM, MOD, OB, T2, S, PR, L, ATT, RX,
    load_sem, ag_send, ag_recv, mp_send, mp_recv, ms_send, ms_recv, cx_send, cx_recv,
    halo_send, halo_recv, aa_send, aa_recv,
):
    z, y, x, c = (lax.axis_index(a) for a in ("z", "y", "x", "c"))
    sp, tp = z * 4 + y, x * 2 + c
    right, left, opp, mate = (x + 1) % 4, (x + 3) % 4, (x + 2) % 4, 1 - c

    def sp_dev(s):
        return (s // 4, s % 4, x, c)

    def tp_dev(t):
        return (z, y, t // 2, t % 2)

    loads = [
        pltpu.make_async_copy(resid.at[pl.ds(0, HALF)], G.at[tp * 2], load_sem.at[0]),
        pltpu.make_async_copy(resid.at[pl.ds(HALF, HALF)], G.at[tp * 2 + 1], load_sem.at[1]),
        pltpu.make_async_copy(context, CX, load_sem.at[2]),
        pltpu.make_async_copy(w_key, WK, load_sem.at[3]),
        pltpu.make_async_copy(w_value, WV, load_sem.at[4]),
        pltpu.make_async_copy(w_query, WQ, load_sem.at[5]),
        pltpu.make_async_copy(w_out, WO, load_sem.at[6]),
    ]
    for one in loads:
        one.start()

    barrier = pltpu.get_barrier_semaphore()

    @pl.loop(1, 8)
    def _(k):
        pl.semaphore_signal(barrier, inc=1, device_id=tp_dev((tp + k) % 8), device_id_type=MESH)

    @pl.loop(1, 16)
    def _(k):
        pl.semaphore_signal(barrier, inc=1, device_id=sp_dev((sp + k) % 16), device_id_type=MESH)

    pl.semaphore_wait(barrier, 22)

    def ag_copy(chunk, slot, device):
        return pltpu.make_async_remote_copy(
            src_ref=G.at[chunk], dst_ref=G.at[chunk], send_sem=ag_send.at[slot],
            recv_sem=ag_recv.at[chunk], device_id=device, device_id_type=MESH,
        )

    to_right, to_left, to_mate = (z, y, right, c), (z, y, left, c), (z, y, x, mate)
    loads[0].wait()
    loads[1].wait()
    ag_copy(tp * 2, 0, to_right).start()
    ag_copy(tp * 2 + 1, 1, to_left).start()
    ag_copy(tp * 2, 2, to_mate).start()
    ag_copy(tp * 2 + 1, 3, to_mate).start()
    ag_copy(tp * 2 + 1, 4, to_right).start()
    ag_copy(tp * 2, 5, to_left).start()

    cf = cond[...].astype(F32)
    lifted = jnp.broadcast_to(cf / (1.0 + jnp.exp(-cf)), (16, 128)).astype(BF16)
    rows8 = lax.broadcasted_iota(jnp.int32, (8, WIDE), 0)
    p_shift = dot(lifted, mod_shift[...])[0:8]
    p_scale = dot(lifted, mod_scale[...])[0:8]
    p_gate = dot(lifted, mod_gate[...])[0:8]
    MP[sp] = jnp.where(rows8 == 0, p_shift, jnp.where(rows8 == 1, p_scale, p_gate))

    def mp_copy(k):
        return pltpu.make_async_remote_copy(
            src_ref=MP.at[sp], dst_ref=MP.at[sp], send_sem=mp_send.at[k],
            recv_sem=mp_recv.at[sp], device_id=sp_dev((sp + k) % 16), device_id_type=MESH,
        )

    def mp_wait(k):
        s = (sp + k) % 16
        return pltpu.make_async_remote_copy(
            src_ref=MP.at[s], dst_ref=MP.at[s], send_sem=mp_send.at[k],
            recv_sem=mp_recv.at[s], device_id=sp_dev(s), device_id_type=MESH,
        )

    @pl.loop(1, 16)
    def _(k):
        mp_copy(k).start()

    loads[2].wait()

    @pl.loop(0, 4)
    def _(i):
        rows = pl.ds(pl.multiple_of(i * 16, 16), 16)
        v = CX[rows, :].astype(F32)
        NRM[rows, :] = (v * inv_rms(v) * norm_gain[...]).astype(BF16)

    loads[3].wait()
    loads[4].wait()
    kg, qg = key_gain[...], query_gain[...]
    ck = dot(NRM[0:64, :], WK[...])
    cv = dot(NRM[0:64, :], WV[...])
    own_ctx = pl.ds(pl.multiple_of(sp * 64, 64), 64)
    for h in range(2):
        part = ck[:, h * HEAD : (h + 1) * HEAD]
        CKV[own_ctx, h * HEAD : (h + 1) * HEAD] = (part * inv_rms(part) * kg).astype(BF16)
    CKV[own_ctx, WIDE:] = cv.astype(BF16)

    def cx_copy(s, k):
        rows = pl.ds(pl.multiple_of(s * 64, 64), 64)
        return pltpu.make_async_remote_copy(
            src_ref=CKV.at[rows], dst_ref=CKV.at[rows], send_sem=cx_send.at[k],
            recv_sem=cx_recv.at[s], device_id=sp_dev((sp + k) % 16), device_id_type=MESH,
        )

    @pl.loop(1, 16)
    def _(k):
        cx_copy(sp, k).start()

    @pl.loop(1, 16)
    def _(k):
        mp_wait(k).wait_recv()

    total = MP[0]
    for s in range(1, 16):
        total = total + MP[s]
    MS[tp] = total

    def ms_copy(t, k):
        return pltpu.make_async_remote_copy(
            src_ref=MS.at[t], dst_ref=MS.at[t], send_sem=ms_send.at[k],
            recv_sem=ms_recv.at[t], device_id=tp_dev((tp + k) % 8), device_id_type=MESH,
        )

    @pl.loop(1, 8)
    def _(k):
        ms_copy(tp, k).start()

    OB[...] = jnp.zeros_like(OB)
    for h in range(2):
        OB[h, 0:15, 0:31] = offset_bias[h] * LOG2E
    col = lax.broadcasted_iota(jnp.int32, (GRID_W, 128), 0)
    lane = lax.broadcasted_iota(jnp.int32, (GRID_W, 128), 1)
    key_col = lane % GRID_W
    begin = jnp.clip(col - 8, 0, GRID_W - 16)
    valid = (key_col >= begin) & (key_col < begin + 16)
    for h in range(2):

        @pl.loop(0, 14)
        def _(o):
            one = jnp.broadcast_to(OB[h, pl.ds(o, 1), :], (GRID_W, 128))
            two = jnp.broadcast_to(OB[h, pl.ds(o + 1, 1), :], (GRID_W, 128))
            one = pltpu.roll(one, 113, 1, stride=1, stride_axis=0)
            two = pltpu.roll(two, 49, 1, stride=1, stride_axis=0)
            T2[h, o] = jnp.where(valid, jnp.where(lane < GRID_W, one, two), NEG)

    @pl.loop(1, 8)
    def _(k):
        ms_copy((tp + k) % 8, k).wait_recv()

    for t in range(8):
        cols = slice(t * WIDE, (t + 1) * WIDE)
        block = MS[t]
        MOD[0:1, cols] = block[0:1]
        MOD[1:2, cols] = norm_gain[:, cols] * (1.0 + block[1:2])
        MOD[2:3, cols] = block[2:3]

    loads[5].wait()

    @pl.loop(0, 4)
    def _(r):
        flip = jnp.where(r == 2, 1, 0)

        def chunk_of(j):
            side = j % 2
            dx = jnp.where(r == 0, 0, jnp.where(r == 3, 2, 3 - 2 * side))
            core = c if j < 2 else mate
            return (((x + dx) % 4) * 2 + core) * 2 + (side + flip) % 2

        @pl.when(r > 0)
        def _():
            for j in range(2):
                chunk = chunk_of(j)
                ag_copy(chunk, 0, to_right).wait_recv()
                ag_copy(chunk, 6 + 2 * r + j, to_mate).start()
                @pl.when(r == 1)
                def _():
                    ag_copy(chunk, 6 + j, to_right if j == 0 else to_left).start()

        for j in range(4):
            chunk = chunk_of(j)
            if j >= 2:
                ag_copy(chunk, 0, to_right).wait_recv()

            @pl.loop(0, 6)
            def _(i):
                rows = pl.ds(pl.multiple_of(i * 16, 16), 16)
                v = G[chunk, rows, :].astype(F32)
                v = v * inv_rms(v) * MOD[1:2, :] + MOD[0:1, :]
                NRM[pl.ds(pl.multiple_of(j * HALF + i * 16, 16), 16), :] = v.astype(BF16)

        for k, w in enumerate((WQ, WK, WV)):
            R[:, k * WIDE : (k + 1) * WIDE] = dot(NRM[...], w[...])
        for j in range(4):
            chunk = chunk_of(j)

            @pl.loop(0, 6)
            def _(i):
                rows = pl.ds(pl.multiple_of(j * HALF + i * 16, 16), 16)
                q_rows = pl.ds(pl.multiple_of(chunk * HALF + i * 16, 16), 16)
                k_rows = pl.ds(pl.multiple_of(chunk * HALF + i * 16 + 4 * GRID_W, 16), 16)
                for h in range(2):
                    a, b = h * HEAD, (h + 1) * HEAD
                    part = R[rows, a:b]
                    Q[q_rows, a:b] = (part * inv_rms(part) * qg).astype(BF16)
                    part = R[rows, WIDE + a : WIDE + b]
                    KV[k_rows, a:b] = (part * inv_rms(part) * kg).astype(BF16)
                KV[k_rows, WIDE:] = R[rows, 2 * WIDE :].astype(BF16)

    EDGE = 4 * GRID_W

    def halo_copy(src, dst, k, s):
        return pltpu.make_async_remote_copy(
            src_ref=KV.at[pl.ds(src, EDGE)], dst_ref=KV.at[pl.ds(dst, EDGE)],
            send_sem=halo_send.at[k], recv_sem=halo_recv.at[k],
            device_id=sp_dev(s), device_id_type=MESH,
        )

    halos = (
        halo_copy(EDGE, 28 * GRID_W, 0, (sp + 15) % 16),
        halo_copy(24 * GRID_W, 0, 1, (sp + 1) % 16),
    )
    for one in halos:
        one.start()

    @pl.loop(1, 16)
    def _(k):
        cx_copy((sp + k) % 16, k).wait_recv()

    for one in halos:
        one.wait_recv()

    lo = jnp.where(sp == 0, 4, 0)
    hi = jnp.where(sp == 15, 20, 24)
    factor = HEAD**-0.5 * LOG2E

    def aa_copy(t, src, k):
        return pltpu.make_async_remote_copy(
            src_ref=ATT.at[t], dst_ref=RX.at[src], send_sem=aa_send.at[k],
            recv_sem=aa_recv.at[src], device_id=tp_dev(t), device_id_type=MESH,
        )

    @pl.loop(1, 9)
    def _(k):
        t = (tp + k) % 8
        base = pl.multiple_of(t * SHARD, SHARD)
        for h in range(2):
            a, b = h * HEAD, (h + 1) * HEAD
            cb = context_bias[h] * LOG2E
            S[:, 0:CTX] = dot_nt(Q[pl.ds(base, SHARD), a:b], CKV[:, a:b])
            keys = []
            for i in range(3):
                row = t * 3 + i
                start = jnp.minimum(jnp.maximum(row, lo), hi)
                keys.append((pl.ds(pl.multiple_of(start * GRID_W, GRID_W), 512), start - row + 3))
                S[i * 64 : (i + 1) * 64, CTX:] = dot_nt(
                    Q[pl.ds(base + i * 64, 64), a:b], KV[keys[i][0], a:b]
                )
            for i in range(3):
                offset = keys[i][1]

                @pl.loop(0, 4)
                def _(j):
                    rows = pl.ds(pl.multiple_of(i * 64 + j * 16, 16), 16)
                    sub = pl.ds(pl.multiple_of(j * 16, 16), 16)
                    zc = S[rows, 0:CTX] * factor
                    bias = jnp.concatenate([T2[h, offset + 2 * n, sub, :] for n in range(4)], axis=1)
                    zw = S[rows, CTX:] * factor + bias
                    top = jnp.maximum(
                        jnp.max(zc, axis=1, keepdims=True) + cb, jnp.max(zw, axis=1, keepdims=True)
                    )
                    pc = jnp.exp2(zc - (top - cb))
                    pw = jnp.exp2(zw - top)
                    norm = jnp.sum(pc, axis=1, keepdims=True) + jnp.sum(pw, axis=1, keepdims=True)
                    PR[rows, 0:CTX] = pc.astype(BF16)
                    PR[rows, CTX:] = pw.astype(BF16)
                    L[rows, :] = jnp.broadcast_to(1.0 / norm, (16, HEAD))

            acc = dot(PR[:, 0:CTX], CKV[:, WIDE + a : WIDE + b])
            for i in range(3):
                part = slice(i * 64, (i + 1) * 64)
                full = acc[part] + dot(PR[part, CTX:], KV[keys[i][0], WIDE + a : WIDE + b])
                ATT[t, part, a:b] = (full * L[part, :]).astype(BF16)

        @pl.when(k < 8)
        def _():
            aa_copy(t, tp, k).start()

    @pl.loop(1, 8)
    def _(k):
        aa_copy(tp, (tp + k) % 8, k).wait_recv()

    RX[tp] = ATT[tp]
    loads[6].wait()

    @pl.loop(0, 8)
    def _(n):
        cols = pl.ds(pl.multiple_of(n * WIDE, WIDE), WIDE)
        acc = dot(RX[0], WO[0:WIDE, cols])
        for t in range(1, 8):
            acc = acc + dot(RX[t], WO[t * WIDE : (t + 1) * WIDE, cols])
        for s in range(2):
            part = slice(s * HALF, (s + 1) * HALF)
            own = G[tp * 2 + s, :, cols].astype(F32)
            out[part, cols] = (own + MOD[2:3, cols] * acc[part]).astype(BF16)

    for slot in range(14):
        ag_copy(tp * 2, slot, to_mate).wait_send()

    @pl.loop(1, 16)
    def _(k):
        mp_copy(k).wait_send()
        cx_copy(sp, k).wait_send()

    @pl.loop(1, 8)
    def _(k):
        ms_copy(tp, k).wait_send()
        aa_copy((tp + k) % 8, tp, k).wait_send()

    for one in halos:
        one.wait_send()


def shards(
    resid, cond, mod_shift, mod_scale, mod_gate, norm_gain, context, w_query, w_key, w_value,
    query_gain, key_gain, offset_bias, context_bias, w_out,
):
    vmem = pl.BlockSpec(memory_space=pltpu.VMEM)
    smem = pl.BlockSpec(memory_space=pltpu.SMEM)
    hbm = pl.BlockSpec(memory_space=pl.ANY)
    dma = pltpu.SemaphoreType.DMA
    scratch = [
        pltpu.VMEM((16, HALF, D), BF16),
        pltpu.VMEM((D, WIDE), BF16),
        pltpu.VMEM((D, WIDE), BF16),
        pltpu.VMEM((D, WIDE), BF16),
        pltpu.VMEM((D, D), BF16),
        pltpu.VMEM((64, D), BF16),
        pltpu.VMEM((4 * HALF, D), BF16),
        pltpu.VMEM((4 * HALF, 3 * WIDE), F32),
        pltpu.VMEM((TOK, WIDE), BF16),
        pltpu.VMEM((TOK + 512, 2 * WIDE), BF16),
        pltpu.VMEM((CTX, 2 * WIDE), BF16),
        pltpu.VMEM((16, 8, WIDE), F32),
        pltpu.VMEM((8, 8, WIDE), F32),
        pltpu.VMEM((8, WIDE), F32),
        pltpu.VMEM((8, D), F32),
        pltpu.VMEM((2, 16, 128), F32),
        pltpu.VMEM((2, 14, GRID_W, 128), F32),
        pltpu.VMEM((SHARD, CTX + 512), F32),
        pltpu.VMEM((SHARD, CTX + 512), BF16),
        pltpu.VMEM((SHARD, HEAD), F32),
        pltpu.VMEM((8, SHARD, WIDE), BF16),
        pltpu.VMEM((8, SHARD, WIDE), BF16),
        dma((7,)), dma((14,)), dma((16,)), dma((16,)), dma((16,)), dma((8,)), dma((8,)),
        dma((16,)), dma((16,)), dma((2,)), dma((2,)), dma((8,)), dma((8,)),
    ]
    return pl.pallas_call(
        kernel,
        out_shape=jax.ShapeDtypeStruct((SHARD, D), BF16),
        in_specs=[hbm, vmem, vmem, vmem, vmem, vmem, hbm, hbm, hbm, hbm, vmem, vmem, vmem, smem, hbm],
        out_specs=vmem,
        scratch_shapes=scratch,
        compiler_params=pltpu.CompilerParams(
            collective_id=0, has_side_effects=True, vmem_limit_bytes=60 * 1024 * 1024
        ),
    )(
        resid, cond.reshape(1, -1), mod_shift, mod_scale, mod_gate, norm_gain.reshape(1, -1),
        context, w_query, w_key, w_value, query_gain.reshape(1, -1), key_gain.reshape(1, -1),
        offset_bias, context_bias, w_out,
    )


def solution(mesh):
    grid = Mesh(mesh.devices.reshape(4, 4, 4, 2), ("z", "y", "x", "c"))
    sp, tp, both = ("z", "y"), ("x", "c"), ("z", "y", "x", "c")
    placed = (
        P(both, None), P(sp), P(sp, tp), P(sp, tp), P(sp, tp), P(), P(sp, None),
        P(None, tp), P(None, tp), P(None, tp), P(), P(), P(tp, None, None), P(tp), P(),
    )
    return jax.shard_map(
        shards, mesh=grid, in_specs=placed, out_specs=P(both, None), check_vma=False
    )
```

time: 250 us -> 120 us (0.48); the launches traced: 245 us -> 120 us
  Pallas kernels: 0 us -> 116 us
  local copies, waits for them, and re-layouts: 64 us -> 3.41 us
  blocking collectives: 53.6 us -> 0 us
  matrix products: 48.4 us -> 0 us
  other arithmetic: 40.8 us -> 0 us
  waiting for transfers between devices: 18.4 us -> 0 us
  between operations: 14.7 us -> 0.01 us
  starting transfers between devices: 5.16 us -> 0 us
    pallas_call x0 -> x1, Pallas kernels: none -> 116 us  [shards(): pl.pallas_call(kernel, out_shape=jax.ShapeDtypeStruct((SHARD, D), BF16),...]
    dot_general x46 -> x0, matrix products: 46.4 us -> none  [the longest x3 10.2 us: attend_rows(): jnp.einsum('nir,hrj,ckj->nhcik', row_onehot, offset_bias, col_onehot, pre...]
    psum x2 -> x0, blocking collectives: 19.5 us -> none  [over_axes(): return functools.reduce(lax.psum, axes, shard)]
    all_gather x1 -> x0, blocking collectives: 17.6 us -> none  [gather_turned(): filled = lax.all_gather(both, axis, axis=0, tiled=True)]
    all_to_all x1 -> x0, blocking collectives: 16.5 us -> none  [shards(): lax.all_to_all(attended, 'tp', split_axis=0, concat_axis=1, tiled=True)]
    slice x13 -> x0, local copies, waits for them, and re-layouts: 16.5 us -> none  [the longest x1 8.02 us: shards(): padded[upper + i:upper + i + middle, :, 1]]
    all_gather x2 -> x0, waiting for transfers between devices: 16.2 us -> none  [the longest x1 16.2 us: shards(): piece = lax.all_gather(normed, 'tp', axis=0, tiled=True)]
    dot_general x2 -> x0, local copies, waits for them, and re-layouts: 15.4 us -> none  [attend_rows(): jnp.einsum('nir,hrj,ckj->nhcik', row_onehot, offset_bias, col_onehot, pre...]
  transfers between devices with their start and end apart: 4 -> 0, of which waited for: 2 -> 0; matrix products, arithmetic and copies ran while one was open for 16% -> 0% of each run, Pallas kernels for 0% -> 0%
where the time goes in v1:
time: 120 us
  Pallas kernels  116 us (97%)
  local copies, waits for them, and re-layouts  3.41 us (3%)
    pallas_call x1, Pallas kernels, shards(): pl.pallas_call(kernel, out_shape=jax.ShapeDtypeStruct((SHARD, D), BF16),...  116 us
    unnamed x2, local copies, waits for them, and re-layouts  3.41 us

profile of v1, /device:TPU:1, one launch (start us, length us, event | category | flops | bytes accessed | tf_op | source)
XLA Modules:
  0.0 119.5 jit_solution(7151048940996037340)
XLA Ops:
  0.0 1.3 %copy.16.offset_bias = f32[2,15,31]{2,1,0:T(8,128)} copy(f32[2,15,31]{2,0,1:T(2,128)} %param.27) | data formatting | bytes 7440 | tf_op args[12]
  1.3 116.1 %shard_map.145 = bf16[192,2048]{1,0:T(8,128)(2,1)} custom-call(bf16[192,2048]{1,0:T(8,128)(2,1)} %resid.1, bf16[1,128]{1,0:T(2,128)(2,1)} %bitcast.5, bf16[128,256]{1,0:T(8,128)(2,1)} %mod_shift.1, bf16[128,256]{1,0:T(8,128)(2,1)} %mod_scale.1, bf16[128,256]{1,0:T(8,128)(2,1)} %mod_gate.1, f32[1,2048]{1,0:T(1,128)} %bitcast.4, bf16[64,2048]{1,0:T(8,128)(2,1)} %context.1, ...), custom_call_target="tpu_custom_call" | custom-call | tf_op jit(solution)/shard_map/pallas_call | solution.py:400
  117.4 2.1 %copy.18 = bf16[192,2048]{1,0:T(8,128)(2,1)} copy(bf16[192,2048]{1,0:T(8,128)(2,1)} %shard_map.145) | data formatting | bytes 1572864

commit v2 on v1

v2 whole, which is shorter than its diff:
```python
import functools

import jax
import jax.numpy as jnp
from jax import lax
from jax.experimental import pallas as pl
from jax.experimental.pallas import tpu as pltpu
from jax.sharding import Mesh
from jax.sharding import PartitionSpec as P

MESH = pl.DeviceIdType.MESH
BF16, F32 = jnp.bfloat16, jnp.float32
EPS = 1e-06
LOG2E = 1.4426950408889634
HEAD = 128
GRID_W = 64
D = 2048
CTX = 1024
ROWS_DEV = 24
TOK = 1536
SHARD = 192
HALF = 96
QUART = 48
WIDE = 256
NEG = -1e30
NT = (((1,), (1,)), ((), ()))


def dot_nt(a, b):
    return lax.dot_general(a, b, NT, preferred_element_type=F32)


def dot(a, b):
    return jnp.dot(a, b, preferred_element_type=F32)


def inv_rms(v):
    return lax.rsqrt(jnp.mean(v * v, axis=-1, keepdims=True) + EPS)


def kernel(
    resid, cond, mod_shift, mod_scale, mod_gate, norm_gain, context, w_query, w_key, w_value,
    query_gain, key_gain, offset_bias, context_bias, w_out, out,
    G, WQ, WK, WV, WO, CX, NRM, R, Q, KV, CKV, MP, MS, MSUM, MOD, OB, T2, S, PR, M, L2, L, ATT, RX,
    load_sem, ag_send, ag_recv, mp_send, mp_recv, ms_send, ms_recv, cx_send, cx_recv,
    halo_send, halo_recv, aa_send, aa_recv,
):
    z, y, x, c = (lax.axis_index(a) for a in ("z", "y", "x", "c"))
    sp, tp = z * 4 + y, x * 2 + c
    right, left, opp, mate = (x + 1) % 4, (x + 3) % 4, (x + 2) % 4, 1 - c

    def sp_dev(s):
        return (s // 4, s % 4, x, c)

    def tp_dev(t):
        return (z, y, t // 2, t % 2)

    with jax.named_scope("entry"):
        loads = [
            pltpu.make_async_copy(
                resid.at[pl.ds(n * QUART, QUART)], G.at[tp * 4 + n], load_sem.at[n]
            )
            for n in range(4)
        ] + [
            pltpu.make_async_copy(context, CX, load_sem.at[4]),
            pltpu.make_async_copy(w_key, WK, load_sem.at[5]),
            pltpu.make_async_copy(w_value, WV, load_sem.at[6]),
            pltpu.make_async_copy(w_query, WQ, load_sem.at[7]),
            pltpu.make_async_copy(w_out, WO, load_sem.at[8]),
        ]
        for one in loads:
            one.start()

        barrier = pltpu.get_barrier_semaphore()

        @pl.loop(1, 8)
        def _(k):
            pl.semaphore_signal(barrier, inc=1, device_id=tp_dev((tp + k) % 8), device_id_type=MESH)

        @pl.loop(1, 16)
        def _(k):
            pl.semaphore_signal(barrier, inc=1, device_id=sp_dev((sp + k) % 16), device_id_type=MESH)

        pl.semaphore_wait(barrier, 22)

    def ag_copy(chunk, slot, device):
        return pltpu.make_async_remote_copy(
            src_ref=G.at[chunk], dst_ref=G.at[chunk], send_sem=ag_send.at[slot],
            recv_sem=ag_recv.at[chunk], device_id=device, device_id_type=MESH,
        )

    to_right, to_left, to_mate = (z, y, right, c), (z, y, left, c), (z, y, x, mate)
    to_right, to_left, to_mate = (z, y, right, c), (z, y, left, c), (z, y, x, mate)
    own = tp * 4
    for n in range(4):
        loads[n].wait()
    ag_copy(own, 0, to_right).start()
    ag_copy(own + 3, 4, to_left).start()
    for n in range(4):
        ag_copy(own + n, 8 + n, to_mate).start()

    cf = cond[...].astype(F32)
    lifted = jnp.broadcast_to(cf / (1.0 + jnp.exp(-cf)), (16, 128)).astype(BF16)
    rows8 = lax.broadcasted_iota(jnp.int32, (8, WIDE), 0)
    p_shift = dot(lifted, mod_shift[...])[0:8]
    p_scale = dot(lifted, mod_scale[...])[0:8]
    p_gate = dot(lifted, mod_gate[...])[0:8]
    MP[sp] = jnp.where(rows8 == 0, p_shift, jnp.where(rows8 == 1, p_scale, p_gate))

    def mp_copy(k):
        return pltpu.make_async_remote_copy(
            src_ref=MP.at[sp], dst_ref=MP.at[sp], send_sem=mp_send.at[k],
            recv_sem=mp_recv.at[sp], device_id=sp_dev((sp + k) % 16), device_id_type=MESH,
        )

    def mp_wait(k):
        s = (sp + k) % 16
        return pltpu.make_async_remote_copy(
            src_ref=MP.at[s], dst_ref=MP.at[s], send_sem=mp_send.at[k],
            recv_sem=mp_recv.at[s], device_id=sp_dev(s), device_id_type=MESH,
        )

    @pl.loop(1, 16)
    def _(k):
        mp_copy(k).start()

    loads[4].wait()

    @pl.loop(0, 4)
    def _(i):
        rows = pl.ds(pl.multiple_of(i * 16, 16), 16)
        v = CX[rows, :].astype(F32)
        NRM[rows, :] = (v * inv_rms(v) * norm_gain[...]).astype(BF16)

    loads[5].wait()
    loads[6].wait()
    kg, qg = key_gain[...], query_gain[...]
    ck = dot(NRM[0:64, :], WK[...])
    cv = dot(NRM[0:64, :], WV[...])
    own_ctx = pl.ds(pl.multiple_of(sp * 64, 64), 64)
    for h in range(2):
        part = ck[:, h * HEAD : (h + 1) * HEAD]
        CKV[own_ctx, h * HEAD : (h + 1) * HEAD] = (part * inv_rms(part) * kg).astype(BF16)
    CKV[own_ctx, WIDE:] = cv.astype(BF16)

    def cx_copy(s, k):
        rows = pl.ds(pl.multiple_of(s * 64, 64), 64)
        return pltpu.make_async_remote_copy(
            src_ref=CKV.at[rows], dst_ref=CKV.at[rows], send_sem=cx_send.at[k],
            recv_sem=cx_recv.at[s], device_id=sp_dev((sp + k) % 16), device_id_type=MESH,
        )

    @pl.loop(1, 16)
    def _(k):
        cx_copy(sp, k).start()

    with jax.named_scope("mp_wait"):
        @pl.loop(1, 16)
        def _(k):
            mp_wait(k).wait_recv()

    total = MP[0]
    for s in range(1, 16):
        total = total + MP[s]
    MS[tp] = total

    def ms_copy(t, k):
        return pltpu.make_async_remote_copy(
            src_ref=MS.at[t], dst_ref=MS.at[t], send_sem=ms_send.at[k],
            recv_sem=ms_recv.at[t], device_id=tp_dev((tp + k) % 8), device_id_type=MESH,
        )

    @pl.loop(1, 8)
    def _(k):
        ms_copy(tp, k).start()

    for n in range(1, 4):
        ag_copy(own + n, n, to_right).start()
        ag_copy(own + 3 - n, 4 + n, to_left).start()

    with jax.named_scope("bias"):
        OB[...] = jnp.zeros_like(OB)
        for h in range(2):
            OB[h, 0:15, 0:31] = offset_bias[:, h, :] * LOG2E
        col = lax.broadcasted_iota(jnp.int32, (GRID_W, 128), 0)
        lane = lax.broadcasted_iota(jnp.int32, (GRID_W, 128), 1)
        key_col = lane % GRID_W
        begin = jnp.clip(col - 8, 0, GRID_W - 16)
        valid = (key_col >= begin) & (key_col < begin + 16)
        for h in range(2):

            @pl.loop(0, 14)
            def _(o):
                one = jnp.broadcast_to(OB[h, pl.ds(o, 1), :], (GRID_W, 128))
                two = jnp.broadcast_to(OB[h, pl.ds(o + 1, 1), :], (GRID_W, 128))
                one = pltpu.roll(one, 113, 1, stride=1, stride_axis=0)
                two = pltpu.roll(two, 49, 1, stride=1, stride_axis=0)
                T2[h, o] = jnp.where(valid, jnp.where(lane < GRID_W, one, two), NEG)

    with jax.named_scope("ms_wait"):
        @pl.loop(1, 8)
        def _(k):
            ms_copy((tp + k) % 8, k).wait_recv()

    for t in range(8):
        cols = slice(t * WIDE, (t + 1) * WIDE)
        block = MS[t]
        MOD[0:1, cols] = block[0:1]
        MOD[1:2, cols] = norm_gain[:, cols] * (1.0 + block[1:2])
        MOD[2:3, cols] = block[2:3]

    loads[7].wait()

    def norm_rows(chunk, at):
        for i in range(HALF // 16):
            v = G[chunk * 2 + i // 3, i % 3 * 16 : i % 3 * 16 + 16, :].astype(F32)
            L[i * 16 : i * 16 + 16, :] = jnp.broadcast_to(inv_rms(v), (16, HEAD))
        for i in range(HALF // 16):
            v = G[chunk * 2 + i // 3, i % 3 * 16 : i % 3 * 16 + 16, :].astype(F32)
            v = v * L[i * 16 : i * 16 + 16, 0:1] * MOD[1:2, :] + MOD[0:1, :]
            NRM[at + i * 16 : at + i * 16 + 16, :] = v.astype(BF16)

    def head_rows(chunk, at):
        for i in range(HALF // 16):
            rows = slice(at + i * 16, at + i * 16 + 16)
            q_rows = pl.ds(pl.multiple_of(chunk * HALF + i * 16, 16), 16)
            k_rows = pl.ds(pl.multiple_of(chunk * HALF + i * 16 + 4 * GRID_W, 16), 16)
            for h in range(2):
                a, b = h * HEAD, (h + 1) * HEAD
                part = R[rows, a:b]
                Q[q_rows, a:b] = (part * inv_rms(part) * qg).astype(BF16)
                part = R[rows, WIDE + a : WIDE + b]
                KV[k_rows, a:b] = (part * inv_rms(part) * kg).astype(BF16)
            KV[k_rows, WIDE:] = R[rows, 2 * WIDE :].astype(BF16)

    @pl.loop(0, 4)
    def _(r):
        flip = jnp.where(r == 2, 1, 0)

        def chunk_of(j):
            side = j % 2
            dx = jnp.where(r == 0, 0, jnp.where(r == 3, 2, 3 - 2 * side))
            core = c if j < 2 else mate
            return (((x + dx) % 4) * 2 + core) * 2 + (side + flip) % 2

        @pl.when(r > 0)
        def _():
            for n in range(2):
                for j in range(2):
                    piece = chunk_of(j) * 2 + (n + j) % 2
                    with jax.named_scope("ring_wait"):
                        ag_copy(piece, 0, to_right).wait_recv()
                    ag_copy(piece, 8 + 4 * r + 2 * j + n, to_mate).start()

                    @pl.when(r == 1)
                    def _():
                        ag_copy(piece, 24 + 2 * j + n, to_right if j == 0 else to_left).start()

        for j in range(4):
            chunk = chunk_of(j)
            if j >= 2:
                with jax.named_scope("mate_wait"):
                    for n in range(2):
                        ag_copy(chunk * 2 + n, 0, to_right).wait_recv()

            norm_rows(chunk, j * HALF)

        with jax.named_scope("qkv"):
            for k, w in enumerate((WQ, WK, WV)):
                R[:, k * WIDE : (k + 1) * WIDE] = dot(NRM[...], w[...])
        for j in range(4):
            head_rows(chunk_of(j), j * HALF)

    EDGE = 4 * GRID_W

    def halo_copy(src, dst, k, s):
        return pltpu.make_async_remote_copy(
            src_ref=KV.at[pl.ds(src, EDGE)], dst_ref=KV.at[pl.ds(dst, EDGE)],
            send_sem=halo_send.at[k], recv_sem=halo_recv.at[k],
            device_id=sp_dev(s), device_id_type=MESH,
        )

    halos = (
        halo_copy(EDGE, 28 * GRID_W, 0, (sp + 15) % 16),
        halo_copy(24 * GRID_W, 0, 1, (sp + 1) % 16),
    )
    for one in halos:
        one.start()

    with jax.named_scope("halo_wait"):
        @pl.loop(1, 16)
        def _(k):
            cx_copy((sp + k) % 16, k).wait_recv()

        for one in halos:
            one.wait_recv()

    lo = jnp.where(sp == 0, 4, 0)
    hi = jnp.where(sp == 15, 20, 24)
    factor = HEAD**-0.5 * LOG2E

    def aa_copy(t, src, k):
        return pltpu.make_async_remote_copy(
            src_ref=ATT.at[t], dst_ref=RX.at[src], send_sem=aa_send.at[k],
            recv_sem=aa_recv.at[src], device_id=tp_dev(t), device_id_type=MESH,
        )

    def lanes(v, op):
        parts = [v[:, n * 128 : (n + 1) * 128] for n in range(v.shape[1] // 128)]
        while len(parts) > 1:
            parts = [op(p, q) for p, q in zip(parts[::2], parts[1::2])] + parts[len(parts) & ~1 :]
        return parts[0]

    def attend(t):
        base = pl.multiple_of(t * SHARD, SHARD)
        keys, offsets = [], []
        for i in range(3):
            row = t * 3 + i
            start = jnp.minimum(jnp.maximum(row, lo), hi)
            keys.append(pl.ds(pl.multiple_of(start * GRID_W, GRID_W), 512))
            offsets.append(start - row + 3)
        for h in range(2):
            a, b = h * HEAD, (h + 1) * HEAD
            S[h, :, 0:CTX] = dot_nt(Q[pl.ds(base, SHARD), a:b], CKV[:, a:b])
            for i in range(3):
                S[h, i * 64 : (i + 1) * 64, CTX:] = dot_nt(
                    Q[pl.ds(base + i * 64, 64), a:b], KV[keys[i], a:b]
                )
        for h in range(2):
            a, b = h * HEAD, (h + 1) * HEAD
            cb = context_bias[h] * LOG2E
            strips = [(i, i * 64 + j * 16, slice(j * 16, j * 16 + 16)) for i in range(3) for j in range(4)]

            def window(i, at, sub):
                bias = [T2[h, offsets[i] + 2 * n, sub, :] for n in range(4)]
                return S[h, at : at + 16, CTX:] * factor + jnp.concatenate(bias, axis=1)

            for i, at, sub in strips:
                top = lanes(S[h, at : at + 16, 0:CTX], jnp.maximum) * factor + cb
                top = jnp.maximum(top, lanes(window(i, at, sub), jnp.maximum))
                M[h, at : at + 16, :] = jnp.broadcast_to(jnp.max(top, axis=1, keepdims=True), (16, 128))
            for i, at, sub in strips:
                top = M[h, at : at + 16, 0:1]
                pc = jnp.exp2(S[h, at : at + 16, 0:CTX] * factor - (top - cb))
                pw = jnp.exp2(window(i, at, sub) - top)
                PR[h, at : at + 16, 0:CTX] = pc.astype(BF16)
                PR[h, at : at + 16, CTX:] = pw.astype(BF16)
                norm = lanes(pc, jnp.add) + lanes(pw, jnp.add)
                norm = jnp.sum(norm, axis=1, keepdims=True)
                L2[h, at : at + 16, :] = jnp.broadcast_to(1.0 / norm, (16, 128))
            acc = dot(PR[h, :, 0:CTX], CKV[:, WIDE + a : WIDE + b])
            for i in range(3):
                part = slice(i * 64, (i + 1) * 64)
                full = acc[part] + dot(PR[h, part, CTX:], KV[keys[i], WIDE + a : WIDE + b])
                ATT[t, part, a:b] = (full * L2[h, part, :]).astype(BF16)

    with jax.named_scope("attention"):
        @pl.loop(1, 9)
        def _(k):
            t = (tp + k) % 8
            attend(t)

            @pl.when(k < 8)
            def _():
                aa_copy(t, tp, k).start()

    with jax.named_scope("aa_wait"):
        @pl.loop(1, 8)
        def _(k):
            aa_copy(tp, (tp + k) % 8, k).wait_recv()

    RX[tp] = ATT[tp]
    loads[8].wait()

    with jax.named_scope("project"):
        @pl.loop(0, 8)
        def _(n):
            cols = pl.ds(pl.multiple_of(n * WIDE, WIDE), WIDE)
            acc = dot(RX[0], WO[0:WIDE, cols])
            for t in range(1, 8):
                acc = acc + dot(RX[t], WO[t * WIDE : (t + 1) * WIDE, cols])
            for s in range(4):
                part = slice(s * QUART, (s + 1) * QUART)
                mine = G[own + s, :, cols].astype(F32)
                out[part, cols] = (mine + MOD[2:3, cols] * acc[part]).astype(BF16)

    with jax.named_scope("drain"):
        for slot in range(28):
            ag_copy(own, slot, to_mate).wait_send()

        @pl.loop(1, 16)
        def _(k):
            mp_copy(k).wait_send()
            cx_copy(sp, k).wait_send()

        @pl.loop(1, 8)
        def _(k):
            ms_copy(tp, k).wait_send()
            aa_copy((tp + k) % 8, tp, k).wait_send()

        for one in halos:
            one.wait_send()


def shards(
    resid, cond, mod_shift, mod_scale, mod_gate, norm_gain, context, w_query, w_key, w_value,
    query_gain, key_gain, offset_bias, context_bias, w_out,
):
    vmem = pl.BlockSpec(memory_space=pltpu.VMEM)
    smem = pl.BlockSpec(memory_space=pltpu.SMEM)
    hbm = pl.BlockSpec(memory_space=pl.ANY)
    dma = pltpu.SemaphoreType.DMA
    scratch = [
        pltpu.VMEM((32, QUART, D), BF16),
        pltpu.VMEM((D, WIDE), BF16),
        pltpu.VMEM((D, WIDE), BF16),
        pltpu.VMEM((D, WIDE), BF16),
        pltpu.VMEM((D, D), BF16),
        pltpu.VMEM((64, D), BF16),
        pltpu.VMEM((4 * HALF, D), BF16),
        pltpu.VMEM((4 * HALF, 3 * WIDE), F32),
        pltpu.VMEM((TOK, WIDE), BF16),
        pltpu.VMEM((TOK + 512, 2 * WIDE), BF16),
        pltpu.VMEM((CTX, 2 * WIDE), BF16),
        pltpu.VMEM((16, 8, WIDE), F32),
        pltpu.VMEM((8, 8, WIDE), F32),
        pltpu.VMEM((8, WIDE), F32),
        pltpu.VMEM((8, D), F32),
        pltpu.VMEM((2, 16, 128), F32),
        pltpu.VMEM((2, 14, GRID_W, 128), F32),
        pltpu.VMEM((2, SHARD, CTX + 512), F32),
        pltpu.VMEM((2, SHARD, CTX + 512), BF16),
        pltpu.VMEM((2, SHARD, HEAD), F32),
        pltpu.VMEM((2, SHARD, HEAD), F32),
        pltpu.VMEM((SHARD, HEAD), F32),
        pltpu.VMEM((8, SHARD, WIDE), BF16),
        pltpu.VMEM((8, SHARD, WIDE), BF16),
        dma((9,)), dma((28,)), dma((32,)), dma((16,)), dma((16,)), dma((8,)), dma((8,)),
        dma((16,)), dma((16,)), dma((2,)), dma((2,)), dma((8,)), dma((8,)),
    ]
    return pl.pallas_call(
        kernel,
        out_shape=jax.ShapeDtypeStruct((SHARD, D), BF16),
        in_specs=[hbm, vmem, vmem, vmem, vmem, vmem, hbm, hbm, hbm, hbm, vmem, vmem, vmem, smem, hbm],
        out_specs=vmem,
        scratch_shapes=scratch,
        compiler_params=pltpu.CompilerParams(
            collective_id=0, has_side_effects=True, vmem_limit_bytes=60 * 1024 * 1024
        ),
    )(
        resid, cond.reshape(1, -1), mod_shift, mod_scale, mod_gate, norm_gain.reshape(1, -1),
        context, w_query, w_key, w_value, query_gain.reshape(1, -1), key_gain.reshape(1, -1),
        jnp.transpose(offset_bias, (1, 0, 2)), context_bias, w_out,
    )


def solution(mesh):
    grid = Mesh(mesh.devices.reshape(4, 4, 4, 2), ("z", "y", "x", "c"))
    sp, tp, both = ("z", "y"), ("x", "c"), ("z", "y", "x", "c")
    placed = (
        P(both, None), P(sp), P(sp, tp), P(sp, tp), P(sp, tp), P(), P(sp, None),
        P(None, tp), P(None, tp), P(None, tp), P(), P(), P(tp, None, None), P(tp), P(),
    )
    return jax.shard_map(
        shards, mesh=grid, in_specs=placed, out_specs=P(both, None), check_vma=False
    )
```

time: 120 us -> 73 us (0.61)
  Pallas kernels: 116 us -> 70.8 us
  local copies, waits for them, and re-layouts: 3.41 us -> 2.09 us
    pallas_call x1, Pallas kernels: 116 us -> 70.8 us  [shards(): pl.pallas_call(kernel, out_shape=jax.ShapeDtypeStruct((SHARD, D), BF16),...]
    unnamed x2 -> x1, local copies, waits for them, and re-layouts: 3.41 us -> 2.09 us
where the time goes in v2:
time: 73 us; the launch traced here: 72.8 us
  Pallas kernels  70.8 us (97%)
  local copies, waits for them, and re-layouts  2.09 us (3%)
    pallas_call x1, Pallas kernels, shards(): pl.pallas_call(kernel, out_shape=jax.ShapeDtypeStruct((SHARD, D), BF16),...  70.8 us
    unnamed x1, local copies, waits for them, and re-layouts  2.09 us

profile of v2, /device:TPU:1, one launch (start us, length us, event | category | flops | bytes accessed | tf_op | source)
XLA Modules:
  0.0 72.8 jit_solution(354014694657897856)
XLA Ops:
  0.0 70.8 %shard_map.145 = bf16[192,2048]{1,0:T(8,128)(2,1)} custom-call(bf16[192,2048]{1,0:T(8,128)(2,1)} %resid.1, bf16[1,128]{1,0:T(2,128)(2,1)} %bitcast.7, bf16[128,256]{1,0:T(8,128)(2,1)} %mod_shift.1, bf16[128,256]{1,0:T(8,128)(2,1)} %mod_scale.1, bf16[128,256]{1,0:T(8,128)(2,1)} %mod_gate.1, f32[1,2048]{1,0:T(1,128)} %bitcast.6, bf16[64,2048]{1,0:T(8,128)(2,1)} %context.1, ...), custom_call_target="tpu_custom_call" | custom-call | tf_op jit(solution)/shard_map/pallas_call | solution.py:441
  70.8 2.1 %copy.17 = bf16[192,2048]{1,0:T(8,128)(2,1)} copy(bf16[192,2048]{1,0:T(8,128)(2,1)} %shard_map.145) | data formatting | bytes 1572864

commit v3 on v2

--- a/solution.py
+++ b/solution.py
@@ -19,6 +19,7 @@
 ROWS_DEV = 24
 TOK = 1536
 SHARD = 192
+PAD = 288
 HALF = 96
 QUART = 48
 WIDE = 256
@@ -41,7 +42,7 @@
 def kernel(
     resid, cond, mod_shift, mod_scale, mod_gate, norm_gain, context, w_query, w_key, w_value,
     query_gain, key_gain, offset_bias, context_bias, w_out, out,
-    G, WQ, WK, WV, WO, CX, NRM, R, Q, KV, CKV, MP, MS, MSUM, MOD, OB, T2, S, PR, M, L2, L, ATT, RX,
+    G, WQ, WK, WV, WO, CX, NRM, R, Q, KV, CKV, MP, MS, MSUM, MOD, OB, T2, S, PR, SW, PW, VA, CVA, QN, ACC, MC, LC, M, L, PA, ATT, RX,
     load_sem, ag_send, ag_recv, mp_send, mp_recv, ms_send, ms_recv, cx_send, cx_recv,
     halo_send, halo_recv, aa_send, aa_recv,
 ):
@@ -211,178 +212,259 @@
 
     loads[7].wait()
 
-    def norm_rows(chunk, at):
-        for i in range(HALF // 16):
-            v = G[chunk * 2 + i // 3, i % 3 * 16 : i % 3 * 16 + 16, :].astype(F32)
-            L[i * 16 : i * 16 + 16, :] = jnp.broadcast_to(inv_rms(v), (16, HEAD))
-        for i in range(HALF // 16):
-            v = G[chunk * 2 + i // 3, i % 3 * 16 : i % 3 * 16 + 16, :].astype(F32)
-            v = v * L[i * 16 : i * 16 + 16, 0:1] * MOD[1:2, :] + MOD[0:1, :]
-            NRM[at + i * 16 : at + i * 16 + 16, :] = v.astype(BF16)
-
-    def head_rows(chunk, at):
-        for i in range(HALF // 16):
+    lo = jnp.where(sp == 0, 0, -4)
+    hi = jnp.where(sp == 15, 16, 20)
+    factor = HEAD**-0.5 * LOG2E
+    STRIPS = range(0, SHARD, 16)
+
+    def piece_of(s, j):
+        r, n, side = s // 2, s % 2, j % 2
+        dx = jnp.where(r == 0, 0, jnp.where(r == 3, 2, 3 - 2 * side))
+        core = c if j < 2 else mate
+        shift = jnp.where(r == 2, 2, 0)
+        later = n + shift if side == 0 else 3 - n - shift
+        return (((x + dx) % 4) * 2 + core) * 4 + jnp.where(r == 0, 2 * n + side, later)
+
+    def full(v):
+        return jnp.broadcast_to(v, (16, 128))
+
+    def tiles(v):
+        return [v[:, n * 128 : (n + 1) * 128] for n in range(v.shape[1] // 128)]
+
+    def tree(parts, op):
+        while len(parts) > 1:
+            parts = [op(p, q) for p, q in zip(parts[::2], parts[1::2])] + parts[len(parts) & ~1 :]
+        return parts[0]
+
+    def spread(ref, rows, new):
+        ref[rows, 0:HEAD] = new[:, 0:HEAD]
+        ref[rows, HEAD : 2 * HEAD] = jnp.ones_like(new[:, 0:HEAD])
+        ref[rows, 2 * HEAD :] = new[:, HEAD:]
+
+    def split(h, both):
+        out_part, sums = both[:, 0:HEAD], both[:, HEAD:]
+        return (out_part, sums) if h == 0 else (sums, out_part)
+
+    def norm_rows(piece, at):
+        for i in range(3):
+            v = G[piece, i * 16 : i * 16 + 16, :].astype(F32)
+            L[at + i * 16 : at + i * 16 + 16, :] = full(inv_rms(v))
+        for i in range(3):
             rows = slice(at + i * 16, at + i * 16 + 16)
-            q_rows = pl.ds(pl.multiple_of(chunk * HALF + i * 16, 16), 16)
-            k_rows = pl.ds(pl.multiple_of(chunk * HALF + i * 16 + 4 * GRID_W, 16), 16)
+            inv = L[rows, :]
+            for n in range(D // 128):
+                cols = slice(n * 128, (n + 1) * 128)
+                v = G[piece, i * 16 : i * 16 + 16, cols].astype(F32)
+                NRM[rows, cols] = (v * inv * MOD[1:2, cols] + MOD[0:1, cols]).astype(BF16)
+
+    def head_rows(piece, at, slot):
+        for i in range(3):
+            rows = slice(at + i * 16, at + i * 16 + 16)
+            q_rows = pl.ds(pl.multiple_of(piece * QUART + i * 16, 16), 16)
+            k_rows = pl.ds(pl.multiple_of(piece * QUART + i * 16 + PAD, 16), 16)
             for h in range(2):
                 a, b = h * HEAD, (h + 1) * HEAD
                 part = R[rows, a:b]
-                Q[q_rows, a:b] = (part * inv_rms(part) * qg).astype(BF16)
+                part = (part * inv_rms(part) * qg).astype(BF16)
+                Q[q_rows, a:b] = part
+                QN[slot, rows, a:b] = part
                 part = R[rows, WIDE + a : WIDE + b]
                 KV[k_rows, a:b] = (part * inv_rms(part) * kg).astype(BF16)
-            KV[k_rows, WIDE:] = R[rows, 2 * WIDE :].astype(BF16)
-
-    @pl.loop(0, 4)
-    def _(r):
-        flip = jnp.where(r == 2, 1, 0)
-
-        def chunk_of(j):
-            side = j % 2
-            dx = jnp.where(r == 0, 0, jnp.where(r == 3, 2, 3 - 2 * side))
-            core = c if j < 2 else mate
-            return (((x + dx) % 4) * 2 + core) * 2 + (side + flip) % 2
-
-        @pl.when(r > 0)
-        def _():
-            for n in range(2):
-                for j in range(2):
-                    piece = chunk_of(j) * 2 + (n + j) % 2
-                    with jax.named_scope("ring_wait"):
-                        ag_copy(piece, 0, to_right).wait_recv()
-                    ag_copy(piece, 8 + 4 * r + 2 * j + n, to_mate).start()
-
-                    @pl.when(r == 1)
-                    def _():
-                        ag_copy(piece, 24 + 2 * j + n, to_right if j == 0 else to_left).start()
+            new = R[rows, 2 * WIDE :].astype(BF16)
+            KV[k_rows, WIDE:] = new
+            spread(VA, k_rows, new)
+
+    def halo_copy(piece, k):
+        src = pl.multiple_of(piece * QUART + PAD, 16)
+        low = k < 6
+        dst = pl.multiple_of(k * QUART + jnp.where(low, PAD + TOK, -PAD), 16)
+        return pltpu.make_async_remote_copy(
+            src_ref=KV.at[pl.ds(src, QUART)], dst_ref=KV.at[pl.ds(dst, QUART)],
+            send_sem=halo_send.at[k], recv_sem=halo_recv.at[k],
+            device_id=sp_dev((sp + jnp.where(low, 15, 1)) % 16), device_id_type=MESH,
+        )
+
+    def context_part(s, slot):
+        for h in range(2):
+            a, b = h * HEAD, (h + 1) * HEAD
+            S[h] = dot_nt(QN[slot, :, a:b], CKV[:, a:b])
+        for h in range(2):
+            a, b = h * HEAD, (h + 1) * HEAD
+            cb = context_bias[h] * LOG2E
+            pieces = [piece_of(s, j) for j in range(4)]
+
+            def place(at):
+                return pl.ds(pl.multiple_of(pieces[at // QUART] * QUART + at % QUART, 16), 16)
+
+            for at in STRIPS:
+                top = tree(tiles(S[h, at : at + 16, :]), jnp.maximum) * factor + cb
+                MC[h, place(at), :] = full(jnp.max(top, axis=1, keepdims=True))
+            for at in STRIPS:
+                top = MC[h, place(at), :] - cb
+                for n in range(CTX // 128):
+                    cols = slice(n * 128, (n + 1) * 128)
+                    PR[h, at : at + 16, cols] = jnp.exp2(
+                        S[h, at : at + 16, cols] * factor - top
+                    ).astype(BF16)
+            acc, sums = split(h, dot(PR[h], CVA[:, a : a + WIDE]))
+            for j in range(4):
+                rows = pl.ds(pl.multiple_of(pieces[j] * QUART, 16), QUART)
+                ACC[rows, a:b] = acc[j * QUART : (j + 1) * QUART]
+                LC[h, rows, :] = sums[j * QUART : (j + 1) * QUART]
+
+    def window_part(t):
+        base = pl.multiple_of(t * SHARD, SHARD)
+        keys, offsets = [], []
+        for i in range(3):
+            row = t * 3 + i
+            start = jnp.minimum(jnp.maximum(row - 4, lo), hi)
+            keys.append(pl.ds(pl.multiple_of(start * GRID_W + PAD, 32), 512))
+            offsets.append(start - row + 7)
+        for h in range(2):
+            a, b = h * HEAD, (h + 1) * HEAD
+            for i in range(3):
+                SW[h, i * 64 : (i + 1) * 64, :] = dot_nt(
+                    Q[pl.ds(base + i * 64, 64), a:b], KV[keys[i], a:b]
+                )
+        for h in range(2):
+            a, b = h * HEAD, (h + 1) * HEAD
+
+            def scores(at):
+                i, sub = at // 64, slice(at % 64, at % 64 + 16)
+                return [
+                    SW[h, at : at + 16, n * 128 : (n + 1) * 128] * factor
+                    + T2[h, offsets[i] + 2 * n, sub, :]
+                    for n in range(4)
+                ]
+
+            for at in STRIPS:
+                top = jnp.max(tree(scores(at), jnp.maximum), axis=1, keepdims=True)
+                M[h, at : at + 16, :] = jnp.maximum(full(top), MC[h, pl.ds(base + at, 16), :])
+            for at in STRIPS:
+                top = M[h, at : at + 16, :]
+                for n, one in enumerate(scores(at)):
+                    PW[h, at : at + 16, n * 128 : (n + 1) * 128] = jnp.exp2(one - top).astype(BF16)
+            for i in range(3):
+                part, rows = slice(i * 64, (i + 1) * 64), pl.ds(base + i * 64, 64)
+                new, sums = split(h, dot(PW[h, part, :], VA[keys[i], a : a + WIDE]))
+                keep = jnp.exp2(MC[h, rows, :] - M[h, part, :])
+                norm = 1.0 / (sums + LC[h, rows, :] * keep)
+                ATT[t, part, a:b] = ((new + ACC[rows, a:b] * keep) * norm).astype(BF16)
+
+    @pl.loop(0, 8)
+    def _(s):
+        r, n = s // 2, s % 2
+        pieces = [piece_of(s, j) for j in range(4)]
 
         for j in range(4):
-            chunk = chunk_of(j)
             if j >= 2:
                 with jax.named_scope("mate_wait"):
-                    for n in range(2):
-                        ag_copy(chunk * 2 + n, 0, to_right).wait_recv()
-
-            norm_rows(chunk, j * HALF)
+                    ag_copy(pieces[j], 0, to_right).wait_recv()
+            norm_rows(pieces[j], j * QUART)
 
         with jax.named_scope("qkv"):
             for k, w in enumerate((WQ, WK, WV)):
                 R[:, k * WIDE : (k + 1) * WIDE] = dot(NRM[...], w[...])
         for j in range(4):
-            head_rows(chunk_of(j), j * HALF)
-
-    EDGE = 4 * GRID_W
-
-    def halo_copy(src, dst, k, s):
-        return pltpu.make_async_remote_copy(
-            src_ref=KV.at[pl.ds(src, EDGE)], dst_ref=KV.at[pl.ds(dst, EDGE)],
-            send_sem=halo_send.at[k], recv_sem=halo_recv.at[k],
-            device_id=sp_dev(s), device_id_type=MESH,
-        )
-
-    halos = (
-        halo_copy(EDGE, 28 * GRID_W, 0, (sp + 15) % 16),
-        halo_copy(24 * GRID_W, 0, 1, (sp + 1) % 16),
-    )
-    for one in halos:
-        one.start()
-
-    with jax.named_scope("halo_wait"):
-        @pl.loop(1, 16)
-        def _(k):
-            cx_copy((sp + k) % 16, k).wait_recv()
-
-        for one in halos:
-            one.wait_recv()
-
-    lo = jnp.where(sp == 0, 4, 0)
-    hi = jnp.where(sp == 15, 20, 24)
-    factor = HEAD**-0.5 * LOG2E
+            head_rows(pieces[j], j * QUART, n)
+        for j in range(4):
+            piece = pieces[j]
+
+            @pl.when((piece < 6) | (piece >= 26))
+            def _():
+                halo_copy(piece, jnp.where(piece < 6, piece, piece - 20)).start()
+
+        @pl.when((s > 0) & (s < 7))
+        def _():
+            for j in range(2):
+                piece = piece_of(s + 1, j)
+                with jax.named_scope("ring_wait"):
+                    ag_copy(piece, 0, to_right).wait_recv()
+                ag_copy(piece, 8 + 2 * (s + 1) + j, to_mate).start()
+
+                @pl.when((s + 1) // 2 == 1)
+                def _():
+                    ag_copy(piece, 24 + 2 * j + (s + 1) % 2, to_right if j == 0 else to_left).start()
+
+        @pl.when(s == 1)
+        def _():
+            with jax.named_scope("ctx_wait"):
+                @pl.loop(1, 16)
+                def _(k):
+                    cx_copy((sp + k) % 16, k).wait_recv()
+
+            for e in range(0, CTX, 128):
+                spread(CVA, slice(e, e + 128), CKV[e : e + 128, WIDE:])
+
+        with jax.named_scope("ctx_part"):
+            @pl.loop(jnp.where(s < 2, 0, s), jnp.where(s == 0, 0, s + 1))
+            def _(e):
+                context_part(e, e % 2)
 
     def aa_copy(t, src, k):
-        return pltpu.make_async_remote_copy(
-            src_ref=ATT.at[t], dst_ref=RX.at[src], send_sem=aa_send.at[k],
+        half = pl.ds(pl.multiple_of(src % 2 * WIDE, WIDE), WIDE)
+        return pltpu.make_async_remote_copy(
+            src_ref=ATT.at[t], dst_ref=RX.at[src // 2, :, half], send_sem=aa_send.at[k],
             recv_sem=aa_recv.at[src], device_id=tp_dev(t), device_id_type=MESH,
         )
 
-    def lanes(v, op):
-        parts = [v[:, n * 128 : (n + 1) * 128] for n in range(v.shape[1] // 128)]
-        while len(parts) > 1:
-            parts = [op(p, q) for p, q in zip(parts[::2], parts[1::2])] + parts[len(parts) & ~1 :]
-        return parts[0]
-
-    def attend(t):
-        base = pl.multiple_of(t * SHARD, SHARD)
-        keys, offsets = [], []
-        for i in range(3):
-            row = t * 3 + i
-            start = jnp.minimum(jnp.maximum(row, lo), hi)
-            keys.append(pl.ds(pl.multiple_of(start * GRID_W, GRID_W), 512))
-            offsets.append(start - row + 3)
-        for h in range(2):
-            a, b = h * HEAD, (h + 1) * HEAD
-            S[h, :, 0:CTX] = dot_nt(Q[pl.ds(base, SHARD), a:b], CKV[:, a:b])
-            for i in range(3):
-                S[h, i * 64 : (i + 1) * 64, CTX:] = dot_nt(
-                    Q[pl.ds(base + i * 64, 64), a:b], KV[keys[i], a:b]
-                )
-        for h in range(2):
-            a, b = h * HEAD, (h + 1) * HEAD
-            cb = context_bias[h] * LOG2E
-            strips = [(i, i * 64 + j * 16, slice(j * 16, j * 16 + 16)) for i in range(3) for j in range(4)]
-
-            def window(i, at, sub):
-                bias = [T2[h, offsets[i] + 2 * n, sub, :] for n in range(4)]
-                return S[h, at : at + 16, CTX:] * factor + jnp.concatenate(bias, axis=1)
-
-            for i, at, sub in strips:
-                top = lanes(S[h, at : at + 16, 0:CTX], jnp.maximum) * factor + cb
-                top = jnp.maximum(top, lanes(window(i, at, sub), jnp.maximum))
-                M[h, at : at + 16, :] = jnp.broadcast_to(jnp.max(top, axis=1, keepdims=True), (16, 128))
-            for i, at, sub in strips:
-                top = M[h, at : at + 16, 0:1]
-                pc = jnp.exp2(S[h, at : at + 16, 0:CTX] * factor - (top - cb))
-                pw = jnp.exp2(window(i, at, sub) - top)
-                PR[h, at : at + 16, 0:CTX] = pc.astype(BF16)
-                PR[h, at : at + 16, CTX:] = pw.astype(BF16)
-                norm = lanes(pc, jnp.add) + lanes(pw, jnp.add)
-                norm = jnp.sum(norm, axis=1, keepdims=True)
-                L2[h, at : at + 16, :] = jnp.broadcast_to(1.0 / norm, (16, 128))
-            acc = dot(PR[h, :, 0:CTX], CKV[:, WIDE + a : WIDE + b])
-            for i in range(3):
-                part = slice(i * 64, (i + 1) * 64)
-                full = acc[part] + dot(PR[h, part, CTX:], KV[keys[i], WIDE + a : WIDE + b])
-                ATT[t, part, a:b] = (full * L2[h, part, :]).astype(BF16)
-
-    with jax.named_scope("attention"):
-        @pl.loop(1, 9)
-        def _(k):
-            t = (tp + k) % 8
-            attend(t)
-
-            @pl.when(k < 8)
+    first_low = jnp.where(tp == 0, 1, 0)
+    near = jnp.where(x < 2, 1, 3)
+
+    with jax.named_scope("window"):
+        @pl.loop(0, 8)
+        def _(k):
+            far = (k < 4) & (k % 2 == 0)
+            dx = jnp.where(k >= 6, 0, jnp.where(far, 2, jnp.where(k < 4, near, 4 - near)))
+            core = jnp.where(k == 6, mate, jnp.where(k == 7, c, jnp.where(k < 4, k // 2, k - 4)))
+            t = (x + dx) % 4 * 2 + core
+
+            @pl.when(t == first_low)
+            def _():
+                with jax.named_scope("halo_low"):
+                    for n in range(6, 12):
+                        halo_copy(n + 20, n).wait_recv()
+                spread(VA, slice(0, PAD), KV[0:PAD, WIDE:])
+
+            @pl.when(t == 7)
+            def _():
+                with jax.named_scope("halo_high"):
+                    for n in range(6):
+                        halo_copy(n, n).wait_recv()
+                spread(VA, slice(PAD + TOK, 2 * PAD + TOK), KV[PAD + TOK :, WIDE:])
+
+            window_part(t)
+
+            @pl.when(k < 7)
             def _():
                 aa_copy(t, tp, k).start()
 
-    with jax.named_scope("aa_wait"):
-        @pl.loop(1, 8)
-        def _(k):
-            aa_copy(tp, (tp + k) % 8, k).wait_recv()
-
-    RX[tp] = ATT[tp]
+    own_half = pl.ds(pl.multiple_of(c * WIDE, WIDE), WIDE)
+    RX[x, :, own_half] = ATT[tp]
     loads[8].wait()
 
-    with jax.named_scope("project"):
-        @pl.loop(0, 8)
-        def _(n):
-            cols = pl.ds(pl.multiple_of(n * WIDE, WIDE), WIDE)
-            acc = dot(RX[0], WO[0:WIDE, cols])
-            for t in range(1, 8):
-                acc = acc + dot(RX[t], WO[t * WIDE : (t + 1) * WIDE, cols])
-            for s in range(4):
-                part = slice(s * QUART, (s + 1) * QUART)
-                mine = G[own + s, :, cols].astype(F32)
-                out[part, cols] = (mine + MOD[2:3, cols] * acc[part]).astype(BF16)
+    for g, dx in enumerate((3, 0, 1, 2)):
+        chip = (x + dx) % 4
+        with jax.named_scope("aa_wait"):
+            if g != 1:
+                aa_copy(tp, chip * 2, 0).wait_recv()
+                aa_copy(tp, chip * 2 + 1, 0).wait_recv()
+            else:
+                aa_copy(tp, x * 2 + mate, 0).wait_recv()
+        with jax.named_scope("project"):
+            for n in range(8):
+                cols = slice(n * WIDE, (n + 1) * WIDE)
+                rows = pl.ds(pl.multiple_of(chip * 2 * WIDE, 2 * WIDE), 2 * WIDE)
+                part = dot(RX[chip], WO[rows, cols])
+                if g > 0:
+                    part = part + PA[:, cols]
+                if g < 3:
+                    PA[:, cols] = part
+                else:
+                    for s in range(4):
+                        some = slice(s * QUART, (s + 1) * QUART)
+                        mine = G[own + s, :, cols].astype(F32)
+                        out[some, cols] = (mine + MOD[2:3, cols] * part[some]).astype(BF16)
 
     with jax.named_scope("drain"):
         for slot in range(28):
@@ -396,10 +478,10 @@
         @pl.loop(1, 8)
         def _(k):
             ms_copy(tp, k).wait_send()
-            aa_copy((tp + k) % 8, tp, k).wait_send()
-
-        for one in halos:
-            one.wait_send()
+            aa_copy(tp, tp, k - 1).wait_send()
+
+        for n in range(12):
+            halo_copy(0, n).wait_send()
 
 
 def shards(
@@ -417,10 +499,10 @@
         pltpu.VMEM((D, WIDE), BF16),
         pltpu.VMEM((D, D), BF16),
         pltpu.VMEM((64, D), BF16),
-        pltpu.VMEM((4 * HALF, D), BF16),
-        pltpu.VMEM((4 * HALF, 3 * WIDE), F32),
+        pltpu.VMEM((SHARD, D), BF16),
+        pltpu.VMEM((SHARD, 3 * WIDE), F32),
         pltpu.VMEM((TOK, WIDE), BF16),
-        pltpu.VMEM((TOK + 512, 2 * WIDE), BF16),
+        pltpu.VMEM((TOK + 2 * PAD, 2 * WIDE), BF16),
         pltpu.VMEM((CTX, 2 * WIDE), BF16),
         pltpu.VMEM((16, 8, WIDE), F32),
         pltpu.VMEM((8, 8, WIDE), F32),
@@ -428,15 +510,23 @@
         pltpu.VMEM((8, D), F32),
         pltpu.VMEM((2, 16, 128), F32),
         pltpu.VMEM((2, 14, GRID_W, 128), F32),
-        pltpu.VMEM((2, SHARD, CTX + 512), F32),
-        pltpu.VMEM((2, SHARD, CTX + 512), BF16),
-        pltpu.VMEM((2, SHARD, HEAD), F32),
+        pltpu.VMEM((2, SHARD, CTX), F32),
+        pltpu.VMEM((2, SHARD, CTX), BF16),
+        pltpu.VMEM((2, SHARD, 512), F32),
+        pltpu.VMEM((2, SHARD, 512), BF16),
+        pltpu.VMEM((TOK + 2 * PAD, 3 * HEAD), BF16),
+        pltpu.VMEM((CTX, 3 * HEAD), BF16),
+        pltpu.VMEM((2, SHARD, WIDE), BF16),
+        pltpu.VMEM((TOK, WIDE), F32),
+        pltpu.VMEM((2, TOK, HEAD), F32),
+        pltpu.VMEM((2, TOK, HEAD), F32),
         pltpu.VMEM((2, SHARD, HEAD), F32),
         pltpu.VMEM((SHARD, HEAD), F32),
+        pltpu.VMEM((SHARD, D), F32),
         pltpu.VMEM((8, SHARD, WIDE), BF16),
-        pltpu.VMEM((8, SHARD, WIDE), BF16),
+        pltpu.VMEM((4, SHARD, 2 * WIDE), BF16),
         dma((9,)), dma((28,)), dma((32,)), dma((16,)), dma((16,)), dma((8,)), dma((8,)),
-        dma((16,)), dma((16,)), dma((2,)), dma((2,)), dma((8,)), dma((8,)),
+        dma((16,)), dma((16,)), dma((12,)), dma((12,)), dma((8,)), dma((8,)),
     ]
     return pl.pallas_call(
         kernel,

time: 73 us -> 62.9 us (0.86)
  Pallas kernels: 70.8 us -> 60.7 us
    pallas_call x1, Pallas kernels: 70.8 us -> 60.7 us  [shards(): pl.pallas_call(kernel, out_shape=jax.ShapeDtypeStruct((SHARD, D), BF16),...]
where the time goes in v3:
time: 62.9 us; the launch traced here: 62.7 us
  Pallas kernels  60.7 us (97%)
  local copies, waits for them, and re-layouts  2.09 us (3%)
    pallas_call x1, Pallas kernels, shards(): pl.pallas_call(kernel, out_shape=jax.ShapeDtypeStruct((SHARD, D), BF16),...  60.7 us
    unnamed x1, local copies, waits for them, and re-layouts  2.09 us

profile of v3, /device:TPU:1, one launch (start us, length us, event | category | flops | bytes accessed | tf_op | source)
XLA Modules:
  0.0 62.7 jit_solution(3151955865827604832)
XLA Ops:
  0.0 60.7 %shard_map.145 = bf16[192,2048]{1,0:T(8,128)(2,1)} custom-call(bf16[192,2048]{1,0:T(8,128)(2,1)} %resid.1, bf16[1,128]{1,0:T(2,128)(2,1)} %bitcast.7, bf16[128,256]{1,0:T(8,128)(2,1)} %mod_shift.1, bf16[128,256]{1,0:T(8,128)(2,1)} %mod_scale.1, bf16[128,256]{1,0:T(8,128)(2,1)} %mod_gate.1, f32[1,2048]{1,0:T(1,128)} %bitcast.6, bf16[64,2048]{1,0:T(8,128)(2,1)} %context.1, ...), custom_call_target="tpu_custom_call" | custom-call | tf_op jit(solution)/shard_map/pallas_call | solution.py:531
  60.7 2.1 %copy.17 = bf16[192,2048]{1,0:T(8,128)(2,1)} copy(bf16[192,2048]{1,0:T(8,128)(2,1)} %shard_map.145) | data formatting | bytes 1572864

commit v4 on v3

--- a/solution.py
+++ b/solution.py
@@ -42,9 +42,9 @@
 def kernel(
     resid, cond, mod_shift, mod_scale, mod_gate, norm_gain, context, w_query, w_key, w_value,
     query_gain, key_gain, offset_bias, context_bias, w_out, out,
-    G, WQ, WK, WV, WO, CX, NRM, R, Q, KV, CKV, MP, MS, MSUM, MOD, OB, T2, S, PR, SW, PW, VA, CVA, QN, ACC, MC, LC, M, L, PA, ATT, RX,
+    G, WQ, WK, WV, WO, CX, NRM, R, Q, KV, CK, CV, MP, MS, MSUM, MOD, OB, T2, S, PR, SW, PW, VA, CVA, QN, ACC, MC, LC, M, L, PA, RL, ATT, RX,
     load_sem, ag_send, ag_recv, mp_send, mp_recv, ms_send, ms_recv, cx_send, cx_recv,
-    halo_send, halo_recv, aa_send, aa_recv,
+    halo_send, halo_recv, aa_send, aa_recv, rl_send, rl_recv,
 ):
     z, y, x, c = (lax.axis_index(a) for a in ("z", "y", "x", "c"))
     sp, tp = z * 4 + y, x * 2 + c
@@ -82,6 +82,14 @@
         def _(k):
             pl.semaphore_signal(barrier, inc=1, device_id=sp_dev((sp + k) % 16), device_id_type=MESH)
 
+        cf = cond[...].astype(F32)
+        lifted = jnp.broadcast_to(cf / (1.0 + jnp.exp(-cf)), (16, 128)).astype(BF16)
+        rows8 = lax.broadcasted_iota(jnp.int32, (8, WIDE), 0)
+        p_shift = dot(lifted, mod_shift[...])[0:8]
+        p_scale = dot(lifted, mod_scale[...])[0:8]
+        p_gate = dot(lifted, mod_gate[...])[0:8]
+        MP[sp] = jnp.where(rows8 == 0, p_shift, jnp.where(rows8 == 1, p_scale, p_gate))
+
         pl.semaphore_wait(barrier, 22)
 
     def ag_copy(chunk, slot, device):
@@ -100,14 +108,6 @@
     for n in range(4):
         ag_copy(own + n, 8 + n, to_mate).start()
 
-    cf = cond[...].astype(F32)
-    lifted = jnp.broadcast_to(cf / (1.0 + jnp.exp(-cf)), (16, 128)).astype(BF16)
-    rows8 = lax.broadcasted_iota(jnp.int32, (8, WIDE), 0)
-    p_shift = dot(lifted, mod_shift[...])[0:8]
-    p_scale = dot(lifted, mod_scale[...])[0:8]
-    p_gate = dot(lifted, mod_gate[...])[0:8]
-    MP[sp] = jnp.where(rows8 == 0, p_shift, jnp.where(rows8 == 1, p_scale, p_gate))
-
     def mp_copy(k):
         return pltpu.make_async_remote_copy(
             src_ref=MP.at[sp], dst_ref=MP.at[sp], send_sem=mp_send.at[k],
@@ -138,22 +138,34 @@
     kg, qg = key_gain[...], query_gain[...]
     ck = dot(NRM[0:64, :], WK[...])
     cv = dot(NRM[0:64, :], WV[...])
-    own_ctx = pl.ds(pl.multiple_of(sp * 64, 64), 64)
+    key_rows = pl.ds(pl.multiple_of(sp * 64, 64), 64)
     for h in range(2):
         part = ck[:, h * HEAD : (h + 1) * HEAD]
-        CKV[own_ctx, h * HEAD : (h + 1) * HEAD] = (part * inv_rms(part) * kg).astype(BF16)
-    CKV[own_ctx, WIDE:] = cv.astype(BF16)
-
-    def cx_copy(s, k):
-        rows = pl.ds(pl.multiple_of(s * 64, 64), 64)
-        return pltpu.make_async_remote_copy(
-            src_ref=CKV.at[rows], dst_ref=CKV.at[rows], send_sem=cx_send.at[k],
-            recv_sem=cx_recv.at[s], device_id=sp_dev((sp + k) % 16), device_id_type=MESH,
-        )
-
-    @pl.loop(1, 16)
-    def _(k):
-        cx_copy(sp, k).start()
+        CK[key_rows, h * HEAD : (h + 1) * HEAD] = (part * inv_rms(part) * kg).astype(BF16)
+    CV[pl.ds(pl.multiple_of((y * 4 + z) * 64, 64), 64), :] = cv.astype(BF16)
+
+    def cx_copy(leg, source, o):
+        along_y = leg in (0, 3)
+        ref, count = (CK, CV, CK, CV)[leg], 64 if leg < 2 else 256
+        at = (source, source, source, source)[leg] * count + (0 if leg > 1 else (z, y)[leg] * 256)
+        rows = pl.ds(pl.multiple_of(at, 64), count)
+        return pltpu.make_async_remote_copy(
+            src_ref=ref.at[rows], dst_ref=ref.at[rows], send_sem=cx_send.at[leg * 4 + o],
+            recv_sem=cx_recv.at[leg * 4 + source],
+            device_id=(z, (y + o) % 4, x, c) if along_y else ((z + o) % 4, y, x, c),
+            device_id_type=MESH,
+        )
+
+    def cx_start(leg):
+        for o in (2, 1, 3):
+            cx_copy(leg, y if leg in (0, 3) else z, o).start()
+
+    def cx_wait(leg):
+        for o in (1, 3, 2):
+            cx_copy(leg, ((y if leg in (0, 3) else z) + o) % 4, o).wait_recv()
+
+    cx_start(0)
+    cx_start(1)
 
     with jax.named_scope("mp_wait"):
         @pl.loop(1, 16)
@@ -178,6 +190,11 @@
     for n in range(1, 4):
         ag_copy(own + n, n, to_right).start()
         ag_copy(own + 3 - n, 4 + n, to_left).start()
+
+    with jax.named_scope("ctx_turn"):
+        for leg in range(2):
+            cx_wait(leg)
+            cx_start(leg + 2)
 
     with jax.named_scope("bias"):
         OB[...] = jnp.zeros_like(OB)
@@ -284,33 +301,30 @@
             device_id=sp_dev((sp + jnp.where(low, 15, 1)) % 16), device_id_type=MESH,
         )
 
-    def context_part(s, slot):
-        for h in range(2):
-            a, b = h * HEAD, (h + 1) * HEAD
-            S[h] = dot_nt(QN[slot, :, a:b], CKV[:, a:b])
-        for h in range(2):
-            a, b = h * HEAD, (h + 1) * HEAD
-            cb = context_bias[h] * LOG2E
-            pieces = [piece_of(s, j) for j in range(4)]
-
-            def place(at):
-                return pl.ds(pl.multiple_of(pieces[at // QUART] * QUART + at % QUART, 16), 16)
-
-            for at in STRIPS:
-                top = tree(tiles(S[h, at : at + 16, :]), jnp.maximum) * factor + cb
-                MC[h, place(at), :] = full(jnp.max(top, axis=1, keepdims=True))
-            for at in STRIPS:
-                top = MC[h, place(at), :] - cb
-                for n in range(CTX // 128):
-                    cols = slice(n * 128, (n + 1) * 128)
-                    PR[h, at : at + 16, cols] = jnp.exp2(
-                        S[h, at : at + 16, cols] * factor - top
-                    ).astype(BF16)
-            acc, sums = split(h, dot(PR[h], CVA[:, a : a + WIDE]))
-            for j in range(4):
-                rows = pl.ds(pl.multiple_of(pieces[j] * QUART, 16), QUART)
-                ACC[rows, a:b] = acc[j * QUART : (j + 1) * QUART]
-                LC[h, rows, :] = sums[j * QUART : (j + 1) * QUART]
+    def context_head(s, h):
+        pieces = [piece_of(s, j) for j in range(4)]
+        a, b = h * HEAD, (h + 1) * HEAD
+        cb = context_bias[h] * LOG2E
+
+        def place(at):
+            return pl.ds(pl.multiple_of(pieces[at // QUART] * QUART + at % QUART, 16), 16)
+
+        S[h] = dot_nt(QN[s % 4, :, a:b], CK[:, a:b])
+        for at in STRIPS:
+            top = tree(tiles(S[h, at : at + 16, :]), jnp.maximum) * factor + cb
+            MC[h, place(at), :] = full(jnp.max(top, axis=1, keepdims=True))
+        for at in STRIPS:
+            top = MC[h, place(at), :] - cb
+            for n in range(CTX // 128):
+                cols = slice(n * 128, (n + 1) * 128)
+                PR[h, at : at + 16, cols] = jnp.exp2(
+                    S[h, at : at + 16, cols] * factor - top
+                ).astype(BF16)
+        acc, sums = split(h, dot(PR[h], CVA[:, a : a + WIDE]))
+        for j in range(4):
+            rows = pl.ds(pl.multiple_of(pieces[j] * QUART, 16), QUART)
+            ACC[rows, a:b] = acc[j * QUART : (j + 1) * QUART]
+            LC[h, rows, :] = sums[j * QUART : (j + 1) * QUART]
 
     def window_part(t):
         base = pl.multiple_of(t * SHARD, SHARD)
@@ -351,99 +365,170 @@
                 norm = 1.0 / (sums + LC[h, rows, :] * keep)
                 ATT[t, part, a:b] = ((new + ACC[rows, a:b] * keep) * norm).astype(BF16)
 
-    @pl.loop(0, 8)
-    def _(s):
-        r, n = s // 2, s % 2
+    def aa_copy(t, src, k):
+        half = pl.ds(pl.multiple_of(src % 2 * WIDE, WIDE), WIDE)
+        return pltpu.make_async_remote_copy(
+            src_ref=ATT.at[t], dst_ref=RX.at[src // 2, :, half], send_sem=aa_send.at[k],
+            recv_sem=aa_recv.at[src], device_id=tp_dev(t), device_id_type=MESH,
+        )
+
+    onward = jnp.where(c == 0, right, left)
+    behind = jnp.where(c == 0, left, right)
+
+    def relay_in(i):
+        return pltpu.make_async_remote_copy(
+            src_ref=ATT.at[opp * 2 + i], dst_ref=RL.at[i], send_sem=rl_send.at[i],
+            recv_sem=rl_recv.at[i], device_id=(z, y, onward, c), device_id_type=MESH,
+        )
+
+    def relay_out(i):
+        half = pl.ds(pl.multiple_of(c * WIDE, WIDE), WIDE)
+        return pltpu.make_async_remote_copy(
+            src_ref=RL.at[i], dst_ref=RX.at[behind, :, half], send_sem=rl_send.at[2 + i],
+            recv_sem=aa_recv.at[behind * 2 + c], device_id=(z, y, onward, i), device_id_type=MESH,
+        )
+
+    first_low = jnp.where(tp == 1, 0, jnp.where(tp == 0, 1, 0))
+    near = jnp.where(x < 2, 1, 3)
+
+    def window(t):
+        @pl.when(t == first_low)
+        def _():
+            with jax.named_scope("halo_low"):
+                for n in range(6, 12):
+                    halo_copy(n + 20, n).wait_recv()
+            spread(VA, slice(0, PAD), KV[0:PAD, WIDE:])
+
+        @pl.when(t == 7)
+        def _():
+            with jax.named_scope("halo_high"):
+                for n in range(6):
+                    halo_copy(n, n).wait_recv()
+            spread(VA, slice(PAD + TOK, 2 * PAD + TOK), KV[PAD + TOK :, WIDE:])
+
+        window_part(t)
+
+    def norm_project(s):
         pieces = [piece_of(s, j) for j in range(4)]
-
+        with jax.named_scope("mate_wait"):
+            for j in (2, 3):
+                ag_copy(pieces[j], 0, to_right).wait_recv()
         for j in range(4):
-            if j >= 2:
-                with jax.named_scope("mate_wait"):
-                    ag_copy(pieces[j], 0, to_right).wait_recv()
             norm_rows(pieces[j], j * QUART)
-
-        with jax.named_scope("qkv"):
-            for k, w in enumerate((WQ, WK, WV)):
-                R[:, k * WIDE : (k + 1) * WIDE] = dot(NRM[...], w[...])
+        for k, w in enumerate((WQ, WK, WV)):
+            R[:, k * WIDE : (k + 1) * WIDE] = dot(NRM[...], w[...])
+
+    def take_next(s):
+        for j in range(2):
+            piece = piece_of(s, j)
+            with jax.named_scope("ring_wait"):
+                ag_copy(piece, 0, to_right).wait_recv()
+            ag_copy(piece, 8 + 2 * s + j, to_mate).start()
+
+            @pl.when(s // 2 == 1)
+            def _():
+                ag_copy(piece, 24 + 2 * j + s % 2, to_right if j == 0 else to_left).start()
+
+    def heads(s):
         for j in range(4):
-            head_rows(pieces[j], j * QUART, n)
+            head_rows(piece_of(s, j), j * QUART, s % 4)
+
+    def send_halo(s):
         for j in range(4):
-            piece = pieces[j]
+            piece = piece_of(s, j)
 
             @pl.when((piece < 6) | (piece >= 26))
             def _():
                 halo_copy(piece, jnp.where(piece < 6, piece, piece - 20)).start()
 
-        @pl.when((s > 0) & (s < 7))
+    @pl.loop(0, 3)
+    def _(s):
+        @pl.when(s > 0)
         def _():
-            for j in range(2):
-                piece = piece_of(s + 1, j)
-                with jax.named_scope("ring_wait"):
-                    ag_copy(piece, 0, to_right).wait_recv()
-                ag_copy(piece, 8 + 2 * (s + 1) + j, to_mate).start()
-
-                @pl.when((s + 1) // 2 == 1)
-                def _():
-                    ag_copy(piece, 24 + 2 * j + (s + 1) % 2, to_right if j == 0 else to_left).start()
-
-        @pl.when(s == 1)
-        def _():
-            with jax.named_scope("ctx_wait"):
-                @pl.loop(1, 16)
-                def _(k):
-                    cx_copy((sp + k) % 16, k).wait_recv()
-
-            for e in range(0, CTX, 128):
-                spread(CVA, slice(e, e + 128), CKV[e : e + 128, WIDE:])
-
-        with jax.named_scope("ctx_part"):
-            @pl.loop(jnp.where(s < 2, 0, s), jnp.where(s == 0, 0, s + 1))
-            def _(e):
-                context_part(e, e % 2)
-
-    def aa_copy(t, src, k):
-        half = pl.ds(pl.multiple_of(src % 2 * WIDE, WIDE), WIDE)
-        return pltpu.make_async_remote_copy(
-            src_ref=ATT.at[t], dst_ref=RX.at[src // 2, :, half], send_sem=aa_send.at[k],
-            recv_sem=aa_recv.at[src], device_id=tp_dev(t), device_id_type=MESH,
-        )
-
-    first_low = jnp.where(tp == 0, 1, 0)
-    near = jnp.where(x < 2, 1, 3)
+            take_next(s + 1)
+
+        with jax.named_scope("first_half"):
+            norm_project(s)
+        with jax.named_scope("second_half"):
+            heads(s)
+        send_halo(s)
+
+    with jax.named_scope("ctx_wait"):
+        cx_wait(2)
+        cx_wait(3)
+
+    for e in range(16):
+        spread(CVA, slice(e * 64, e * 64 + 64), CV[pl.ds((e % 4 * 4 + e // 4) * 64, 64), :])
+    with jax.named_scope("ctx01"):
+        @pl.loop(0, 2)
+        def _(e):
+            context_head(e, 0)
+            context_head(e, 1)
+
+    @pl.loop(3, 6)
+    def _(s):
+        take_next(s + 1)
+        with jax.named_scope("first_half"):
+            norm_project(s)
+            context_head(s - 1, 0)
+        with jax.named_scope("second_half"):
+            heads(s)
+            context_head(s - 1, 1)
+        send_halo(s)
+
+    s6, s7 = tp * 0 + 6, tp * 0 + 7
+    with jax.named_scope("first_half"):
+        norm_project(s6)
+        context_head(5, 0)
+    take_next(s7)
+    with jax.named_scope("second_half"):
+        heads(s6)
+        context_head(5, 1)
+        context_head(6, 0)
+    send_halo(s6)
+    with jax.named_scope("first_half"):
+        norm_project(s7)
+    with jax.named_scope("second_half"):
+        heads(s7)
+    send_halo(s7)
+    with jax.named_scope("ctx7"):
+        context_head(6, 1)
+        context_head(7, 0)
+        context_head(7, 1)
 
     with jax.named_scope("window"):
         @pl.loop(0, 8)
         def _(k):
-            far = (k < 4) & (k % 2 == 0)
-            dx = jnp.where(k >= 6, 0, jnp.where(far, 2, jnp.where(k < 4, near, 4 - near)))
-            core = jnp.where(k == 6, mate, jnp.where(k == 7, c, jnp.where(k < 4, k // 2, k - 4)))
+            home = (k == 4) | (k == 5)
+            middle = (x == 1) | (x == 2)
+            side = jnp.where(middle, jnp.where(k < 4, near, 4 - near), 1 + k % 2 * 2)
+            dx = jnp.where(home, 0, jnp.where(k < 2, 2, side))
+            core = jnp.where(home, (mate + k) % 2, k % 2)
+            core = jnp.where(middle | (k < 6) & (home | (k < 2)), core, k // 4)
             t = (x + dx) % 4 * 2 + core
 
-            @pl.when(t == first_low)
+            @pl.when((k == 5) | (k == 6))
             def _():
-                with jax.named_scope("halo_low"):
-                    for n in range(6, 12):
-                        halo_copy(n + 20, n).wait_recv()
-                spread(VA, slice(0, PAD), KV[0:PAD, WIDE:])
-
-            @pl.when(t == 7)
+                with jax.named_scope("relay_wait"):
+                    relay_in(k - 5).wait_recv()
+                relay_out(k - 5).start()
+
+            window(t)
+
+            @pl.when(k < 2)
             def _():
-                with jax.named_scope("halo_high"):
-                    for n in range(6):
-                        halo_copy(n, n).wait_recv()
-                spread(VA, slice(PAD + TOK, 2 * PAD + TOK), KV[PAD + TOK :, WIDE:])
-
-            window_part(t)
-
-            @pl.when(k < 7)
+                relay_in(k).start()
+
+            @pl.when((k >= 2) & (k != 5))
             def _():
-                aa_copy(t, tp, k).start()
+                aa_copy(t, tp, jnp.where(k < 5, k, k - 1)).start()
 
     own_half = pl.ds(pl.multiple_of(c * WIDE, WIDE), WIDE)
     RX[x, :, own_half] = ATT[tp]
     loads[8].wait()
 
-    for g, dx in enumerate((3, 0, 1, 2)):
+    odd = x % 2
+    for g, dx in enumerate((3 - 2 * odd, 0, 2, 1 + 2 * odd)):
         chip = (x + dx) % 4
         with jax.named_scope("aa_wait"):
             if g != 1:
@@ -473,12 +558,20 @@
         @pl.loop(1, 16)
         def _(k):
             mp_copy(k).wait_send()
-            cx_copy(sp, k).wait_send()
+
+        for leg in range(4):
+            for o in (1, 2, 3):
+                cx_copy(leg, 0, o).wait_send()
 
         @pl.loop(1, 8)
         def _(k):
             ms_copy(tp, k).wait_send()
-            aa_copy(tp, tp, k - 1).wait_send()
+
+        for k in range(2, 7):
+            aa_copy(tp, tp, k).wait_send()
+        for i in range(2):
+            relay_in(i).wait_send()
+            relay_out(i).wait_send()
 
         for n in range(12):
             halo_copy(0, n).wait_send()
@@ -503,7 +596,8 @@
         pltpu.VMEM((SHARD, 3 * WIDE), F32),
         pltpu.VMEM((TOK, WIDE), BF16),
         pltpu.VMEM((TOK + 2 * PAD, 2 * WIDE), BF16),
-        pltpu.VMEM((CTX, 2 * WIDE), BF16),
+        pltpu.VMEM((CTX, WIDE), BF16),
+        pltpu.VMEM((CTX, WIDE), BF16),
         pltpu.VMEM((16, 8, WIDE), F32),
         pltpu.VMEM((8, 8, WIDE), F32),
         pltpu.VMEM((8, WIDE), F32),
@@ -516,17 +610,18 @@
         pltpu.VMEM((2, SHARD, 512), BF16),
         pltpu.VMEM((TOK + 2 * PAD, 3 * HEAD), BF16),
         pltpu.VMEM((CTX, 3 * HEAD), BF16),
-        pltpu.VMEM((2, SHARD, WIDE), BF16),
+        pltpu.VMEM((4, SHARD, WIDE), BF16),
         pltpu.VMEM((TOK, WIDE), F32),
         pltpu.VMEM((2, TOK, HEAD), F32),
         pltpu.VMEM((2, TOK, HEAD), F32),
         pltpu.VMEM((2, SHARD, HEAD), F32),
         pltpu.VMEM((SHARD, HEAD), F32),
         pltpu.VMEM((SHARD, D), F32),
+        pltpu.VMEM((2, SHARD, WIDE), BF16),
         pltpu.VMEM((8, SHARD, WIDE), BF16),
         pltpu.VMEM((4, SHARD, 2 * WIDE), BF16),
         dma((9,)), dma((28,)), dma((32,)), dma((16,)), dma((16,)), dma((8,)), dma((8,)),
-        dma((16,)), dma((16,)), dma((12,)), dma((12,)), dma((8,)), dma((8,)),
+        dma((16,)), dma((16,)), dma((12,)), dma((12,)), dma((8,)), dma((8,)), dma((4,)), dma((2,)),
     ]
     return pl.pallas_call(
         kernel,

time: 62.9 us -> 61.3 us (0.975)
  Pallas kernels: 60.7 us -> 59.1 us
    pallas_call x1, Pallas kernels: 60.7 us -> 59.1 us  [shards(): pl.pallas_call(kernel, out_shape=jax.ShapeDtypeStruct((SHARD, D), BF16),...]
where the time goes in v4:
time: 61.3 us; the launch traced here: 61.1 us
  Pallas kernels  59.1 us (96%)
  local copies, waits for them, and re-layouts  2.09 us (3%)
    pallas_call x1, Pallas kernels, shards(): pl.pallas_call(kernel, out_shape=jax.ShapeDtypeStruct((SHARD, D), BF16),...  59.1 us
    unnamed x1, local copies, waits for them, and re-layouts  2.09 us

profile of v4, /device:TPU:1, one launch (start us, length us, event | category | flops | bytes accessed | tf_op | source)
XLA Modules:
  0.0 61.1 jit_solution(8341938396447064340)
XLA Ops:
  0.0 59.1 %shard_map.145 = bf16[192,2048]{1,0:T(8,128)(2,1)} custom-call(bf16[192,2048]{1,0:T(8,128)(2,1)} %resid.1, bf16[1,128]{1,0:T(2,128)(2,1)} %bitcast.7, bf16[128,256]{1,0:T(8,128)(2,1)} %mod_shift.1, bf16[128,256]{1,0:T(8,128)(2,1)} %mod_scale.1, bf16[128,256]{1,0:T(8,128)(2,1)} %mod_gate.1, f32[1,2048]{1,0:T(1,128)} %bitcast.6, bf16[64,2048]{1,0:T(8,128)(2,1)} %context.1, ...), custom_call_target="tpu_custom_call" | custom-call | tf_op jit(solution)/shard_map/pallas_call | solution.py:626
  59.1 2.1 %copy.17 = bf16[192,2048]{1,0:T(8,128)(2,1)} copy(bf16[192,2048]{1,0:T(8,128)(2,1)} %shard_map.145) | data formatting | bytes 1572864

commit v5 on v4

--- a/solution.py
+++ b/solution.py
@@ -105,6 +105,7 @@
         loads[n].wait()
     ag_copy(own, 0, to_right).start()
     ag_copy(own + 3, 4, to_left).start()
+
     for n in range(4):
         ag_copy(own + n, 8 + n, to_mate).start()
 
@@ -301,7 +302,8 @@
             device_id=sp_dev((sp + jnp.where(low, 15, 1)) % 16), device_id_type=MESH,
         )
 
-    def context_head(s, h):
+    def context_head(s, h, slot=None):
+        slot = h if slot is None else slot
         pieces = [piece_of(s, j) for j in range(4)]
         a, b = h * HEAD, (h + 1) * HEAD
         cb = context_bias[h] * LOG2E
@@ -309,24 +311,24 @@
         def place(at):
             return pl.ds(pl.multiple_of(pieces[at // QUART] * QUART + at % QUART, 16), 16)
 
-        S[h] = dot_nt(QN[s % 4, :, a:b], CK[:, a:b])
+        S[slot] = dot_nt(QN[s % 4, :, a:b], CK[:, a:b])
         for at in STRIPS:
-            top = tree(tiles(S[h, at : at + 16, :]), jnp.maximum) * factor + cb
+            top = tree(tiles(S[slot, at : at + 16, :]), jnp.maximum) * factor + cb
             MC[h, place(at), :] = full(jnp.max(top, axis=1, keepdims=True))
         for at in STRIPS:
             top = MC[h, place(at), :] - cb
             for n in range(CTX // 128):
                 cols = slice(n * 128, (n + 1) * 128)
-                PR[h, at : at + 16, cols] = jnp.exp2(
-                    S[h, at : at + 16, cols] * factor - top
+                PR[slot, at : at + 16, cols] = jnp.exp2(
+                    S[slot, at : at + 16, cols] * factor - top
                 ).astype(BF16)
-        acc, sums = split(h, dot(PR[h], CVA[:, a : a + WIDE]))
+        acc, sums = split(h, dot(PR[slot], CVA[:, a : a + WIDE]))
         for j in range(4):
             rows = pl.ds(pl.multiple_of(pieces[j] * QUART, 16), QUART)
             ACC[rows, a:b] = acc[j * QUART : (j + 1) * QUART]
             LC[h, rows, :] = sums[j * QUART : (j + 1) * QUART]
 
-    def window_part(t):
+    def window_part(t, slot):
         base = pl.multiple_of(t * SHARD, SHARD)
         keys, offsets = [], []
         for i in range(3):
@@ -337,31 +339,30 @@
         for h in range(2):
             a, b = h * HEAD, (h + 1) * HEAD
             for i in range(3):
-                SW[h, i * 64 : (i + 1) * 64, :] = dot_nt(
+                SW[slot + h, i * 64 : (i + 1) * 64, :] = dot_nt(
                     Q[pl.ds(base + i * 64, 64), a:b], KV[keys[i], a:b]
                 )
         for h in range(2):
             a, b = h * HEAD, (h + 1) * HEAD
 
-            def scores(at):
+            for at in STRIPS:
                 i, sub = at // 64, slice(at % 64, at % 64 + 16)
-                return [
-                    SW[h, at : at + 16, n * 128 : (n + 1) * 128] * factor
-                    + T2[h, offsets[i] + 2 * n, sub, :]
-                    for n in range(4)
-                ]
-
+                scores = []
+                for n in range(4):
+                    cols = slice(n * 128, (n + 1) * 128)
+                    scores.append(SW[slot + h, at : at + 16, cols] * factor + T2[h, offsets[i] + 2 * n, sub, :])
+                    SW[slot + h, at : at + 16, cols] = scores[-1]
+                top = jnp.max(tree(scores, jnp.maximum), axis=1, keepdims=True)
+                M[slot + h, at : at + 16, :] = jnp.maximum(full(top), MC[h, pl.ds(base + at, 16), :])
             for at in STRIPS:
-                top = jnp.max(tree(scores(at), jnp.maximum), axis=1, keepdims=True)
-                M[h, at : at + 16, :] = jnp.maximum(full(top), MC[h, pl.ds(base + at, 16), :])
-            for at in STRIPS:
-                top = M[h, at : at + 16, :]
-                for n, one in enumerate(scores(at)):
-                    PW[h, at : at + 16, n * 128 : (n + 1) * 128] = jnp.exp2(one - top).astype(BF16)
+                top = M[slot + h, at : at + 16, :]
+                for n in range(4):
+                    cols = slice(n * 128, (n + 1) * 128)
+                    PW[slot + h, at : at + 16, cols] = jnp.exp2(SW[slot + h, at : at + 16, cols] - top).astype(BF16)
             for i in range(3):
                 part, rows = slice(i * 64, (i + 1) * 64), pl.ds(base + i * 64, 64)
-                new, sums = split(h, dot(PW[h, part, :], VA[keys[i], a : a + WIDE]))
-                keep = jnp.exp2(MC[h, rows, :] - M[h, part, :])
+                new, sums = split(h, dot(PW[slot + h, part, :], VA[keys[i], a : a + WIDE]))
+                keep = jnp.exp2(MC[h, rows, :] - M[slot + h, part, :])
                 norm = 1.0 / (sums + LC[h, rows, :] * keep)
                 ATT[t, part, a:b] = ((new + ACC[rows, a:b] * keep) * norm).astype(BF16)
 
@@ -391,7 +392,7 @@
     first_low = jnp.where(tp == 1, 0, jnp.where(tp == 0, 1, 0))
     near = jnp.where(x < 2, 1, 3)
 
-    def window(t):
+    def halo_wait(t):
         @pl.when(t == first_low)
         def _():
             with jax.named_scope("halo_low"):
@@ -406,17 +407,17 @@
                     halo_copy(n, n).wait_recv()
             spread(VA, slice(PAD + TOK, 2 * PAD + TOK), KV[PAD + TOK :, WIDE:])
 
-        window_part(t)
-
-    def norm_project(s):
-        pieces = [piece_of(s, j) for j in range(4)]
+    def mate_wait(s):
         with jax.named_scope("mate_wait"):
             for j in (2, 3):
-                ag_copy(pieces[j], 0, to_right).wait_recv()
-        for j in range(4):
-            norm_rows(pieces[j], j * QUART)
+                ag_copy(piece_of(s, j), 0, to_right).wait_recv()
+
+    def norm_project(s, which):
+        part = slice(which[0] * QUART, (which[-1] + 1) * QUART)
+        for j in which:
+            norm_rows(piece_of(s, j), j * QUART)
         for k, w in enumerate((WQ, WK, WV)):
-            R[:, k * WIDE : (k + 1) * WIDE] = dot(NRM[...], w[...])
+            R[part, k * WIDE : (k + 1) * WIDE] = dot(NRM[part, :], w[...])
 
     def take_next(s):
         for j in range(2):
@@ -429,8 +430,8 @@
             def _():
                 ag_copy(piece, 24 + 2 * j + s % 2, to_right if j == 0 else to_left).start()
 
-    def heads(s):
-        for j in range(4):
+    def heads(s, which):
+        for j in which:
             head_rows(piece_of(s, j), j * QUART, s % 4)
 
     def send_halo(s):
@@ -440,6 +441,8 @@
             @pl.when((piece < 6) | (piece >= 26))
             def _():
                 halo_copy(piece, jnp.where(piece < 6, piece, piece - 20)).start()
+
+    ALL = (0, 1, 2, 3)
 
     @pl.loop(0, 3)
     def _(s):
@@ -447,10 +450,12 @@
         def _():
             take_next(s + 1)
 
+        mate_wait(s)
         with jax.named_scope("first_half"):
-            norm_project(s)
+            norm_project(s, ALL)
+
         with jax.named_scope("second_half"):
-            heads(s)
+            heads(s, ALL)
         send_halo(s)
 
     with jax.named_scope("ctx_wait"):
@@ -460,47 +465,57 @@
     for e in range(16):
         spread(CVA, slice(e * 64, e * 64 + 64), CV[pl.ds((e % 4 * 4 + e // 4) * 64, 64), :])
     with jax.named_scope("ctx01"):
-        @pl.loop(0, 2)
-        def _(e):
-            context_head(e, 0)
-            context_head(e, 1)
-
-    @pl.loop(3, 6)
+        for e in range(2):
+            for h in range(2):
+                context_head(tp * 0 + e, h, 2 * e + h)
+
+    s3, s7 = tp * 0 + 3, tp * 0 + 7
+    mate_wait(s3)
+    with jax.named_scope("project_s"):
+        norm_project(s3, ALL)
+        heads(s3, ALL)
+    send_halo(s3)
+    take_next(s3 + 1)
+    with jax.named_scope("ctx23"):
+        for e in range(2):
+            for h in range(2):
+                context_head(s3 - 1 + e, h, 2 * e + h)
+
+    @pl.loop(4, 7)
     def _(s):
-        take_next(s + 1)
-        with jax.named_scope("first_half"):
-            norm_project(s)
-            context_head(s - 1, 0)
-        with jax.named_scope("second_half"):
-            heads(s)
-            context_head(s - 1, 1)
+        mate_wait(s)
+        with jax.named_scope("project_s"):
+            norm_project(s, ALL)
+            heads(s, ALL)
         send_halo(s)
 
-    s6, s7 = tp * 0 + 6, tp * 0 + 7
-    with jax.named_scope("first_half"):
-        norm_project(s6)
-        context_head(5, 0)
+        @pl.when(s < 6)
+        def _():
+            take_next(s + 1)
+
+        with jax.named_scope("ctx_s"):
+            context_head(s, 0)
+            context_head(s, 1)
+
     take_next(s7)
-    with jax.named_scope("second_half"):
-        heads(s6)
-        context_head(5, 1)
-        context_head(6, 0)
-    send_halo(s6)
-    with jax.named_scope("first_half"):
-        norm_project(s7)
-    with jax.named_scope("second_half"):
-        heads(s7)
+    with jax.named_scope("last_own"):
+        norm_project(s7, (0, 1))
+        heads(s7, (0, 1))
+    mate_wait(s7)
+    with jax.named_scope("last_mate"):
+        norm_project(s7, (2, 3))
+        heads(s7, (2, 3))
     send_halo(s7)
     with jax.named_scope("ctx7"):
-        context_head(6, 1)
         context_head(7, 0)
         context_head(7, 1)
+
+    middle = (x == 1) | (x == 2)
 
     with jax.named_scope("window"):
         @pl.loop(0, 8)
         def _(k):
             home = (k == 4) | (k == 5)
-            middle = (x == 1) | (x == 2)
             side = jnp.where(middle, jnp.where(k < 4, near, 4 - near), 1 + k % 2 * 2)
             dx = jnp.where(home, 0, jnp.where(k < 2, 2, side))
             core = jnp.where(home, (mate + k) % 2, k % 2)
@@ -513,7 +528,8 @@
                     relay_in(k - 5).wait_recv()
                 relay_out(k - 5).start()
 
-            window(t)
+            halo_wait(t)
+            window_part(t, 0)
 
             @pl.when(k < 2)
             def _():
@@ -521,7 +537,7 @@
 
             @pl.when((k >= 2) & (k != 5))
             def _():
-                aa_copy(t, tp, jnp.where(k < 5, k, k - 1)).start()
+                aa_copy(t, tp, k).start()
 
     own_half = pl.ds(pl.multiple_of(c * WIDE, WIDE), WIDE)
     RX[x, :, own_half] = ATT[tp]
@@ -567,7 +583,7 @@
         def _(k):
             ms_copy(tp, k).wait_send()
 
-        for k in range(2, 7):
+        for k in (2, 3, 4, 6, 7):
             aa_copy(tp, tp, k).wait_send()
         for i in range(2):
             relay_in(i).wait_send()
@@ -604,17 +620,17 @@
         pltpu.VMEM((8, D), F32),
         pltpu.VMEM((2, 16, 128), F32),
         pltpu.VMEM((2, 14, GRID_W, 128), F32),
-        pltpu.VMEM((2, SHARD, CTX), F32),
-        pltpu.VMEM((2, SHARD, CTX), BF16),
-        pltpu.VMEM((2, SHARD, 512), F32),
-        pltpu.VMEM((2, SHARD, 512), BF16),
+        pltpu.VMEM((4, SHARD, CTX), F32),
+        pltpu.VMEM((4, SHARD, CTX), BF16),
+        pltpu.VMEM((4, SHARD, 512), F32),
+        pltpu.VMEM((4, SHARD, 512), BF16),
         pltpu.VMEM((TOK + 2 * PAD, 3 * HEAD), BF16),
         pltpu.VMEM((CTX, 3 * HEAD), BF16),
         pltpu.VMEM((4, SHARD, WIDE), BF16),
         pltpu.VMEM((TOK, WIDE), F32),
         pltpu.VMEM((2, TOK, HEAD), F32),
         pltpu.VMEM((2, TOK, HEAD), F32),
-        pltpu.VMEM((2, SHARD, HEAD), F32),
+        pltpu.VMEM((4, SHARD, HEAD), F32),
         pltpu.VMEM((SHARD, HEAD), F32),
         pltpu.VMEM((SHARD, D), F32),
         pltpu.VMEM((2, SHARD, WIDE), BF16),
@@ -625,7 +641,7 @@
     ]
     return pl.pallas_call(
         kernel,
-        out_shape=jax.ShapeDtypeStruct((SHARD, D), BF16),
+        out_shape=pltpu.VMEM((SHARD, D), BF16),
         in_specs=[hbm, vmem, vmem, vmem, vmem, vmem, hbm, hbm, hbm, hbm, vmem, vmem, vmem, smem, hbm],
         out_specs=vmem,
         scratch_shapes=scratch,

time: 61.3 us -> 59.1 us (0.964)
  local copies, waits for them, and re-layouts: 2.09 us -> 0.88 us
  Pallas kernels: 59.1 us -> 58 us
    unnamed x1, local copies, waits for them, and re-layouts: 2.09 us -> 0.88 us
    pallas_call x1, Pallas kernels: 59.1 us -> 58 us  [shards(): pl.pallas_call(kernel, out_shape=pltpu.VMEM((SHARD, D), BF16), in_specs=[...]
where the time goes in v5:
time: 59.1 us; the launch traced here: 58.9 us
  Pallas kernels  58 us (98%)
  local copies, waits for them, and re-layouts  0.88 us (1%)
    pallas_call x1, Pallas kernels, shards(): pl.pallas_call(kernel, out_shape=pltpu.VMEM((SHARD, D), BF16), in_specs=[...  58 us

profile of v5, /device:TPU:1, one launch (start us, length us, event | category | flops | bytes accessed | tf_op | source)
XLA Modules:
  0.0 58.9 jit_solution(15269520478142107857)
XLA Ops:
  0.0 58.0 %shard_map.145 = bf16[192,2048]{1,0:T(8,128)(2,1)S(1)} custom-call(bf16[192,2048]{1,0:T(8,128)(2,1)} %resid.1, bf16[1,128]{1,0:T(2,128)(2,1)} %bitcast.7, bf16[128,256]{1,0:T(8,128)(2,1)} %mod_shift.1, bf16[128,256]{1,0:T(8,128)(2,1)} %mod_scale.1, bf16[128,256]{1,0:T(8,128)(2,1)} %mod_gate.1, f32[1,2048]{1,0:T(1,128)} %bitcast.6, bf16[64,2048]{1,0:T(8,128)(2,1)} %context.1, ...), custom_call_target="tpu_custom_call" | custom-call | tf_op jit(solution)/shard_map/pallas_call | solution.py:642
  58.0 0.9 %copy.17 = bf16[192,2048]{1,0:T(8,128)(2,1)} copy(bf16[192,2048]{1,0:T(8,128)(2,1)S(1)} %shard_map.145) | data formatting | bytes 1572864
